TPU v7x, 256 devices: a whole 4x4x8 slice. The times are simulated.
256 devices in a mesh: gr: 2 (over z_hi), sp: 16 (over z_lo, y), tp: 8 (over x, core).
Axes of the slice: x: 4, y: 4, z: 8 (z_hi: 2, z_lo: 4; z = z_hi * 4 + z_lo), core: 2. Of those that a mesh axis runs over, the one named last changes fastest.
Arguments:
- prompt: bfloat16 [256, 256, 1024], P('gr', 'sp'), parts along dimension 0, may hold values from -6 to 6
- w_key: bfloat16 [1024, 8, 128], P(None, 'tp'), may hold values from -0.1875 to 0.1875
- w_value: bfloat16 [1024, 8, 128], P(None, 'tp'), may hold values from -0.1875 to 0.1875
- w_in_gate: bfloat16 [2, 1024, 8], P(None, None, 'tp'), may hold values from -0.1875 to 0.1875
- w_forget_gate: bfloat16 [2, 1024, 8], P(None, None, 'tp'), may hold values from -0.1875 to 0.1875
- in_bias: float32 [2, 8], P(None, 'tp'), may hold values from -6 to 0, as said below
- forget_bias: float32 [2, 8], P(None, 'tp'), may hold values from 1 to 10, as said below
- query: bfloat16 [256, 8, 128], P(('gr', 'sp'), 'tp'), parts along dimension 0, may hold values from -6 to 6
- w_out: bfloat16 [8, 128, 1024], P('tp'), may hold values from -0.5 to 0.5
Outputs:
- memory: bfloat16 [2, 256, 8, 128, 128], P(None, ('gr', 'sp'), 'tp'), parts along dimension 1
- normalizer: float32 [2, 256, 8, 128], P(None, ('gr', 'sp'), 'tp'), parts along dimension 1
- stabilizer: float32 [2, 256, 8], P(None, ('gr', 'sp'), 'tp'), parts along dimension 1
- read: bfloat16 [256, 1024], P(('gr', 'sp'), 'tp'), parts along dimension 0
There are 2 independent parts, one for each index of `gr`. A program takes and returns all parts, laid end to end along the dimension named above; an argument that names none is the same for every part. Nothing has to cross between parts.
Inputs may be any that keep to these rules, and one draw needn't show every extreme that they name: forget_bias lies between 1 and 10; the per-head share of memory kept over the whole prompt is spread between a few and some ninety percent. in_bias lies between -6 and 0.
All inputs are finite; a program needn't handle non-finite values.
Results may differ from a plain program's by a relative error of at most 0.015.
Values may be sent and summed in bfloat16 or wider, within the bound.
A program may use at most 64 MiB of HBM per device.

v0:
```python
import functools

import jax
import jax.numpy as jnp
from jax import lax
from jax.experimental import pallas as pl
from jax.experimental.pallas import tpu as pltpu
from jax.sharding import PartitionSpec as P

MESH = pl.DeviceIdType.MESH
F32 = jnp.float32
BF16 = jnp.bfloat16


def nt(a, b):
    return lax.dot_general(a, b, (((1,), (1,)), ((), ())), preferred_element_type=F32)


def kernel(
    n, tpn, heads, width, gates,
    prompt, wk_hbm, wv_hbm, wo_hbm, ig_hbm, fg_hbm, ib_hbm, fb_hbm, q_hbm,
    membuf, norm_out, stab_out, read_out,
    in_gate, forget_gate, in_bias, forget_bias, query, xbuf, raw, wkt, wv, wo, bias, hid, stabs, parts, got,
    wsem, lsem, ssem, rsem, fsend, frecv, xsend, xrecv,
):
    sp = lax.axis_index("sp")
    tp = lax.axis_index("tp")
    seqs, length, _ = xbuf.shape
    rounds = seqs // tpn
    block = length // n
    order = sorted(range(1, n), key=lambda k: abs(k - n / 2))

    barrier = pltpu.get_barrier_semaphore()
    for k in order:
        pl.semaphore_signal(
            barrier, inc=1, device_id={"sp": lax.rem(sp + k, n)}, device_id_type=MESH
        )
    for j in range(1, tpn):
        pl.semaphore_signal(
            barrier, inc=1, device_id={"tp": lax.rem(tp + j, tpn)}, device_id_type=MESH
        )

    weights = [
        pltpu.make_async_copy(wk_hbm, raw.at[0], wsem.at[0]),
        pltpu.make_async_copy(wv_hbm, raw.at[1], wsem.at[1]),
        pltpu.make_async_copy(wo_hbm, wo, wsem.at[2]),
        pltpu.make_async_copy(ig_hbm, in_gate, wsem.at[3]),
        pltpu.make_async_copy(fg_hbm, forget_gate, wsem.at[4]),
        pltpu.make_async_copy(ib_hbm, in_bias, wsem.at[5]),
        pltpu.make_async_copy(fb_hbm, forget_bias, wsem.at[6]),
        pltpu.make_async_copy(q_hbm, query, wsem.at[7]),
    ]
    rows = pl.ds(pl.multiple_of(sp * block, block), block)

    def own(r):
        q = tp * rounds + r
        return pltpu.make_async_copy(prompt.at[sp * seqs + q], xbuf.at[q, rows], lsem.at[r])

    def send(r, k):
        q = tp * rounds + r
        dest = lax.rem(sp + k, n)
        return pltpu.make_async_remote_copy(
            src_ref=prompt.at[dest * seqs + q],
            dst_ref=xbuf.at[q, rows],
            send_sem=ssem.at[r, k],
            recv_sem=rsem.at[r, k],
            device_id={"sp": dest},
            device_id_type=MESH,
        )

    def forward(r, j):
        q = tp * rounds + r
        return pltpu.make_async_remote_copy(
            src_ref=xbuf.at[q],
            dst_ref=xbuf.at[q],
            send_sem=fsend.at[r, j],
            recv_sem=frecv.at[r, j],
            device_id={"tp": lax.rem(tp + j, tpn)},
            device_id_type=MESH,
        )

    for copy in weights:
        copy.start()
    for r in range(rounds):
        own(r).start()
    pl.semaphore_wait(barrier, n - 1 + tpn - 1)
    for r in range(rounds):
        for k in order:
            send(r, k).start()
    stabs[...] = jnp.zeros_like(stabs)
    for copy in weights[3:]:
        copy.wait()
    key_rows = heads * width
    depth = wv.shape[0]

    def gate_rows(ref):
        pieces = [ref[g].astype(F32) for g in range(2)]
        if gates > 2 * heads:
            pieces.append(jnp.zeros((gates - 2 * heads, depth), F32))
        return jnp.concatenate(pieces, axis=0)

    wkt[key_rows:] = jnp.concatenate([gate_rows(in_gate), gate_rows(forget_gate)], axis=0).astype(BF16)
    line = lax.broadcasted_iota(jnp.int32, bias.shape, 0)
    column = jnp.zeros(bias.shape, F32)
    for base, ref in ((0, in_bias), (gates, forget_bias)):
        for g in range(2):
            for h in range(heads):
                column = jnp.where(
                    line == base + g * heads + h, ref[g : g + 1, h : h + 1], column
                )
    bias[...] = column
    weights[0].wait()
    for d in range(0, depth, 128):
        wkt[:key_rows, d : d + 128] = raw[0, d : d + 128].reshape(128, key_rows).T
    weights[1].wait()
    wv[...] = raw[1].reshape(depth, key_rows)
    weights[2].wait()

    tri = (
        lax.broadcasted_iota(jnp.int32, (length, length), 0)
        <= lax.broadcasted_iota(jnp.int32, (length, length), 1)
    ).astype(BF16)
    ahead = lax.broadcasted_iota(jnp.int32, (gates, length), 0) < heads
    lane = lax.broadcasted_iota(jnp.int32, (gates, stabs.shape[1]), 1)
    pick = lax.broadcasted_iota(jnp.int32, (16, length), 0)

    def project(q):
        x = xbuf[q]
        values = jnp.dot(x, wv[...], preferred_element_type=F32).astype(BF16)
        return nt(wkt[...], x), values

    def compute(q, kt, values):
        pre = kt[key_rows:] + bias[...]
        keys = kt[:key_rows].astype(BF16)
        in_log, forget_pre = pre[:gates], pre[gates:]
        forget = jnp.minimum(forget_pre, 0.0) - jnp.log1p(jnp.exp(-jnp.abs(forget_pre)))
        first = forget.astype(BF16).astype(F32)
        second = (forget - first).astype(BF16).astype(F32)
        third = forget - first - second
        pieces = jnp.concatenate([first, second, third, jnp.zeros_like(third)], axis=0)
        sums = jnp.dot(pieces.astype(BF16), tri, preferred_element_type=F32)
        running = sums[:gates] + sums[gates : 2 * gates] + sums[2 * gates : 3 * gates]
        total = running[:, length - 1 :]
        log_weight = in_log + jnp.where(ahead, total - running, running - forget)
        stable = jnp.maximum(total, jnp.max(log_weight, axis=1, keepdims=True))
        weight = jnp.exp(log_weight - stable) * width ** (-0.5)
        floor = jnp.maximum(jnp.exp(-stable), 1.0)
        stabs[...] = jnp.where(lane == q, stable, stabs[...])
        high = weight.astype(BF16).astype(F32)
        split = jnp.concatenate([high, weight - high], axis=0).astype(BF16)
        queries = query[q]
        for h in range(heads):
            head = keys[h * width : (h + 1) * width]
            head_f = head.astype(F32)
            w0, w1 = weight[h : h + 1], weight[heads + h : heads + h + 1]
            scores = jnp.dot(queries, head, preferred_element_type=F32)[h : h + 1]
            q0, q1 = scores * w0, scores * w1
            both = jnp.where(lax.rem(pick, 2) == 0, q0, q1)
            top = both.astype(BF16).astype(F32)
            tail = jnp.where(pick < 2, top, jnp.where(pick < 4, both - top, 0.0)).astype(BF16)
            lhs = jnp.concatenate(
                [(head_f * w0).astype(BF16), (head_f * w1).astype(BF16), tail], axis=0
            )
            res = jnp.dot(
                lhs, values[:, h * width : (h + 1) * width], preferred_element_type=F32
            )
            membuf[0, q, h] = res[:width].astype(BF16)
            membuf[1, q, h] = res[width : 2 * width].astype(BF16)
            normal = nt(split, head)
            normal = normal[:gates] + normal[gates:]
            norm_out[0, q, h : h + 1] = normal[h : h + 1]
            norm_out[1, q, h : h + 1] = normal[heads + h : heads + h + 1]
            last = res[2 * width :]
            d0 = jnp.abs(jnp.sum(q0, axis=1, keepdims=True))
            d1 = jnp.abs(jnp.sum(q1, axis=1, keepdims=True))
            f0, f1 = floor[h : h + 1], floor[heads + h : heads + h + 1]
            hid[q, :, h * width : (h + 1) * width] = (
                (last[0:1] + last[2:3]) / jnp.maximum(d0, f0)
                + (last[1:2] + last[3:4]) / jnp.maximum(d1, f1)
            )

    def turn(r, carry):
        own(r).wait()
        for k in order:
            send(r, k).wait_recv()
        for j in range(1, tpn):
            forward(r, j).start()
        before = (tp * rounds + r, *project(tp * rounds + r))
        for j in range(1, tpn):
            forward(r, j).wait_recv()
            q = lax.rem(tp + tpn - j, tpn) * rounds + r
            after = (q, *project(q))
            compute(*before)
            before = after
        compute(*before)
        return carry

    lax.fori_loop(0, rounds, turn, 0)

    terms = jnp.dot(hid[:, 0, :].astype(BF16), wo[...], preferred_element_type=F32)
    share = terms.shape[1] // tpn
    for t in range(tpn):
        parts[t] = terms[:, t * share : (t + 1) * share]

    def give(j):
        peer = lax.rem(tp + j, tpn)
        return pltpu.make_async_remote_copy(
            src_ref=parts.at[peer],
            dst_ref=got.at[j],
            send_sem=xsend.at[j],
            recv_sem=xrecv.at[j],
            device_id={"tp": peer},
            device_id_type=MESH,
        )

    for j in range(1, tpn):
        give(j).start()
    for g in range(2):
        stab_out[g] = stabs[g * heads : (g + 1) * heads, :seqs]
    for r in range(rounds):
        for k in order:
            send(r, k).wait_send()
        for j in range(1, tpn):
            forward(r, j).wait_send()
    total = parts[tp]
    for j in range(1, tpn):
        give(j).wait()
        total = total + got[j]
    read_out[...] = total.astype(BF16)


def publish(count, *refs):
    sources, targets, sems = refs[:count], refs[count : 2 * count], refs[2 * count]
    copies = [
        pltpu.make_async_copy(a, b, sems.at[i]) for i, (a, b) in enumerate(zip(sources, targets))
    ]
    for copy in copies:
        copy.start()
    for copy in copies:
        copy.wait()


def solution(mesh):
    n, tpn = mesh.shape["sp"], mesh.shape["tp"]

    def body(prompt, w_key, w_value, w_in_gate, w_forget_gate, in_bias, forget_bias, query, w_out):
        depth, heads, width = w_key.shape
        seqs = prompt.shape[0] // n
        length = prompt.shape[1] * n
        rounds = seqs // tpn
        gates = -(-2 * heads // 8) * 8
        wo = w_out.reshape(heads * width, -1)
        columns = wo.shape[1]
        any_ = pl.BlockSpec(memory_space=pl.ANY)
        vmem = pl.BlockSpec(memory_space=pltpu.VMEM)
        dma = pltpu.SemaphoreType.DMA
        shapes = (
            ((2, seqs, heads, width, width), BF16),
            ((2, seqs, heads, width), F32),
            ((2, heads, seqs), F32),
            ((seqs, columns // tpn), BF16),
        )
        held = pl.pallas_call(
            functools.partial(kernel, n, tpn, heads, width, gates),
            out_shape=tuple(pltpu.VMEM(*shape) for shape in shapes),
            in_specs=[any_] * 9,
            out_specs=(vmem,) * 4,
            scratch_shapes=[
                pltpu.VMEM((2, heads, depth), BF16),
                pltpu.VMEM((2, heads, depth), BF16),
                pltpu.VMEM((2, heads), F32),
                pltpu.VMEM((2, heads), F32),
                pltpu.VMEM((seqs, heads, width), BF16),
                pltpu.VMEM((seqs, length, depth), BF16),
                pltpu.VMEM((2, depth, heads, width), BF16),
                pltpu.VMEM((heads * width + 2 * gates, depth), BF16),
                pltpu.VMEM((depth, heads * width), BF16),
                pltpu.VMEM(wo.shape, BF16),
                pltpu.VMEM((2 * gates, length), F32),
                pltpu.VMEM((seqs, 1, heads * width), F32),
                pltpu.VMEM((gates, 128), F32),
                pltpu.VMEM((tpn, seqs, columns // tpn), F32),
                pltpu.VMEM((tpn, seqs, columns // tpn), F32),
                dma((8,)),
                dma((rounds,)),
                dma((rounds, n)),
                dma((rounds, n)),
                dma((rounds, tpn)),
                dma((rounds, tpn)),
                dma((tpn,)),
                dma((tpn,)),
            ],
            compiler_params=pltpu.CompilerParams(collective_id=0, has_side_effects=True),
            name="memories",
        )(
            prompt, w_key, w_value, wo,
            w_in_gate.transpose(0, 2, 1), w_forget_gate.transpose(0, 2, 1),
            in_bias, forget_bias, query,
        )
        memory, normal, stable, read = pl.pallas_call(
            functools.partial(publish, len(shapes)),
            out_shape=tuple(jax.ShapeDtypeStruct(*shape) for shape in shapes),
            in_specs=[vmem] * len(shapes),
            out_specs=(any_,) * len(shapes),
            scratch_shapes=[dma((len(shapes),))],
            name="outputs",
        )(*[pltpu.with_memory_space_constraint(a, pltpu.VMEM) for a in held])
        return memory, normal, stable.transpose(0, 2, 1), read

    return jax.shard_map(
        body,
        mesh=mesh,
        in_specs=(
            P("gr", "sp", None),
            P(None, "tp", None),
            P(None, "tp", None),
            P(None, None, "tp"),
            P(None, None, "tp"),
            P(None, "tp"),
            P(None, "tp"),
            P(("gr", "sp"), "tp", None),
            P("tp", None, None),
        ),
        out_specs=(
            P(None, ("gr", "sp"), "tp", None, None),
            P(None, ("gr", "sp"), "tp", None),
            P(None, ("gr", "sp"), "tp"),
            P(("gr", "sp"), "tp"),
        ),
        check_vma=False,
    )
```

profile of v0, /device:TPU:1, one launch (start us, length us, event | category | flops | bytes accessed | tf_op | source)
XLA Modules:
  0.0 86.2 jit_solution(12910401502523627044)
XLA Ops:
  0.6 1.3 %copy.23.ib_hbm = f32[2,1]{1,0:T(2,128)} copy(f32[2,1]{0,1:T(1,128)} %param.14) | data formatting | bytes 16 | tf_op args[5]
  1.9 1.3 %copy.24.fb_hbm = f32[2,1]{1,0:T(2,128)} copy(f32[2,1]{0,1:T(1,128)} %param.15) | data formatting | bytes 16 | tf_op args[6]
  3.2 1.3 %copy.25.q_hbm = bf16[8,1,128]{2,1,0:T(2,128)(2,1)} copy(bf16[8,1,128]{2,0,1:T(8,128)(2,1)} %param.16) | data formatting | bytes 4096 | tf_op args[7]
  4.5 1.3 %copy.21.ig_hbm = bf16[2,1,1024]{2,1,0:T(2,128)(2,1)} copy(bf16[2,1,1024]{2,0,1:T(2,128)(2,1)} %bitcast.7) | data formatting | bytes 8192 | tf_op jit(solution)/shard_map/transpose | solution.py:297
  5.8 1.3 %copy.22.fg_hbm = bf16[2,1,1024]{2,1,0:T(2,128)(2,1)} copy(bf16[2,1,1024]{2,0,1:T(2,128)(2,1)} %bitcast.8) | data formatting | bytes 8192 | tf_op jit(solution)/shard_map/transpose | solution.py:297
  7.1 2.1 %copy.19.wk_hbm = bf16[1024,1,128]{2,1,0:T(2,128)(2,1)} copy(bf16[1024,1,128]{2,0,1:T(8,128)(2,1)} %param.10) | data formatting | bytes 524288 | tf_op args[1]
  9.2 2.1 %copy.20.wv_hbm = bf16[1024,1,128]{2,1,0:T(2,128)(2,1)} copy(bf16[1024,1,128]{2,0,1:T(8,128)(2,1)} %param.11) | data formatting | bytes 524288 | tf_op args[2]
  11.4 74.0 %memories.1 = (bf16[2,8,1,128,128]{4,3,2,1,0:T(8,128)(2,1)S(1)}, f32[2,8,1,128]{3,2,1,0:T(1,128)S(1)}, f32[2,1,8]{2,1,0:T(1,128)S(1)}, bf16[8,128]{1,0:T(8,128)(2,1)S(1)}) custom-call(bf16[128,16,1024]{2,1,0:T(8,128)(2,1)} %prompt.1, bf16[1024,1,128]{2,1,0:T(2,128)(2,1)} %copy.19.wk_hbm, bf16[1024,1,128]{2,1,0:T(2,128)(2,1)} %copy.20.wv_hbm, ...), custom_call_target="tpu_custom_call" | custom-call | tf_op jit(solution)/shard_map/memories/pallas_call | solution.py:263
  85.4 0.8 outputs.1
where the time goes:
time: 87.2 us; the launch traced here: 86.2 us
  Pallas kernels  74.9 us (86%)
  local copies, waits for them, and re-layouts  10.7 us (12%)
    pallas_call x1, Pallas kernels, body(): pl.pallas_call(functools.partial(kernel, n, tpn, heads, width, gates), ou...  74 us
    unnamed x5, local copies, waits for them, and re-layouts  8.15 us

commit v1 on v0

v1 whole, which is shorter than its diff:
```python
import functools

import jax
import jax.numpy as jnp
from jax import lax
from jax.experimental import pallas as pl
from jax.experimental.pallas import tpu as pltpu
from jax.sharding import PartitionSpec as P

MESH = pl.DeviceIdType.MESH
F32 = jnp.float32
BF16 = jnp.bfloat16
HIGHEST = lax.Precision.HIGHEST


def nt(a, b):
    return lax.dot_general(a, b, (((1,), (1,)), ((), ())), preferred_element_type=F32)


def tn(a, b):
    return lax.dot_general(a, b, (((0,), (0,)), ((), ())), preferred_element_type=F32)


def iota(shape, axis):
    return lax.broadcasted_iota(jnp.int32, shape, axis)


def kernel(
    n, tpn,
    prompt, wk_hbm, wv_hbm, wo_hbm, ig_hbm, fg_hbm, ib_hbm, fb_hbm, q_hbm,
    membuf, norm_out, stab_out, read_out,
    xall, wkv, wo, in_gate, forget_gate, in_bias, forget_bias, query,
    wg, kvs, kvn, kvf, gsend, grecv, xfar, wb, qb, acc, num, nrm, parts, got,
    wsem, lsem, fsend, frecv, nsend, nrecv, gsem, grsem, xsend, xrecv, dsend, drecv, psend, precv,
):
    sp = lax.axis_index("sp")
    tp = lax.axis_index("tp")
    half = n // 2
    cores = 2
    chips = tpn // cores
    seqs, sources, block, depth = xfar.shape
    rows = seqs * block
    width = wo.shape[0]
    side = sp // half
    local = sp - side * half
    near_base = side * half
    far_base = half - near_base
    x, c = tp // cores, lax.rem(tp, cores)
    partner = x * cores + 1 - c

    barrier = pltpu.get_barrier_semaphore()
    for k in range(1, n):
        pl.semaphore_signal(
            barrier, inc=1, device_id={"sp": lax.rem(sp + k, n)}, device_id_type=MESH
        )
    for j in range(1, tpn):
        pl.semaphore_signal(
            barrier, inc=1, device_id={"tp": lax.rem(tp + j, tpn)}, device_id_type=MESH
        )

    weights = [
        pltpu.make_async_copy(wk_hbm, wkv.at[:, :width], wsem.at[0]),
        pltpu.make_async_copy(wv_hbm, wkv.at[:, width:], wsem.at[1]),
        pltpu.make_async_copy(ig_hbm, in_gate, wsem.at[2]),
        pltpu.make_async_copy(fg_hbm, forget_gate, wsem.at[3]),
        pltpu.make_async_copy(ib_hbm, in_bias, wsem.at[4]),
        pltpu.make_async_copy(fb_hbm, forget_bias, wsem.at[5]),
        pltpu.make_async_copy(q_hbm, query, wsem.at[6]),
        pltpu.make_async_copy(wo_hbm, wo, wsem.at[7]),
    ]

    def near_of(k):
        return near_base + lax.rem(local + k, half)

    def far_of(k):
        return far_base + lax.rem(local + k, half)

    def far_from(k):
        return lax.rem(local + half - k, half)

    def load(k):
        return pltpu.make_async_copy(
            prompt.at[pl.ds(near_of(k) * seqs, seqs)],
            xall.at[pl.ds(near_of(k) * seqs, seqs)],
            lsem.at[k],
        )

    def load_far():
        part = pl.ds(far_base * seqs, half * seqs)
        return pltpu.make_async_copy(prompt.at[part], xall.at[part], lsem.at[half])

    def send_far(k):
        dest = far_of(k)
        return pltpu.make_async_remote_copy(
            src_ref=prompt.at[dest * seqs + tp],
            dst_ref=xfar.at[tp, local],
            send_sem=fsend.at[k],
            recv_sem=frecv.at[k],
            device_id={"sp": dest},
            device_id_type=MESH,
        )

    def send_near(k):
        return pltpu.make_async_remote_copy(
            src_ref=kvs.at[k],
            dst_ref=kvn.at[local],
            send_sem=nsend.at[k],
            recv_sem=nrecv.at[k],
            device_id={"sp": near_of(k)},
            device_id_type=MESH,
        )

    def send_gates(k):
        dest = lax.rem(sp + k, n)
        return pltpu.make_async_remote_copy(
            src_ref=gsend.at[dest],
            dst_ref=grecv.at[sp],
            send_sem=gsem.at[k],
            recv_sem=grsem.at[k],
            device_id={"sp": dest},
            device_id_type=MESH,
        )

    def spread(j, k):
        piece = xfar.at[tp, far_from(k)]
        return pltpu.make_async_remote_copy(
            src_ref=piece,
            dst_ref=piece,
            send_sem=xsend.at[j, k],
            recv_sem=xrecv.at[j, k],
            device_id={"tp": lax.rem(x + j, chips) * cores + c},
            device_id_type=MESH,
        )

    def hand(j, k):
        origin = lax.rem(x + chips - j, chips) * cores + c
        piece = xfar.at[origin, far_from(k)]
        return pltpu.make_async_remote_copy(
            src_ref=piece,
            dst_ref=piece,
            send_sem=dsend.at[j, k],
            recv_sem=drecv.at[j, k],
            device_id={"tp": partner},
            device_id_type=MESH,
        )

    def give(j):
        peer = lax.rem(tp + j, tpn)
        return pltpu.make_async_remote_copy(
            src_ref=parts.at[peer],
            dst_ref=got.at[j],
            send_sem=psend.at[j],
            recv_sem=precv.at[j],
            device_id={"tp": peer},
            device_id_type=MESH,
        )

    for copy in weights[:4]:
        copy.start()
    for k in list(range(1, half)) + [0]:
        load(k).start()
    load_far().start()
    for copy in weights[4:]:
        copy.start()
    pl.semaphore_wait(barrier, n - 1 + tpn - 1)
    for k in range(half):
        send_far(k).start()

    for copy in weights[:4]:
        copy.wait()
    wg[...] = jnp.concatenate(
        [in_gate[...].astype(F32), forget_gate[...].astype(F32), jnp.zeros((wg.shape[0] - 4, depth), F32)],
        axis=0,
    ).astype(BF16)

    def rows_of(dest):
        return xall[pl.ds(dest * seqs, seqs)].reshape(rows, depth)

    def gates_to(dest):
        gsend[pl.ds(dest, 1)] = nt(wg[...], rows_of(dest))[: gsend.shape[1]][None]

    for k in list(range(1, half)) + [0]:
        load(k).wait()
        dest = near_of(k)
        both = jnp.dot(rows_of(dest), wkv[...], preferred_element_type=F32).astype(BF16)
        gates_to(dest)
        if k:
            kvs[k] = both
            send_near(k).start()
        else:
            kvn[pl.ds(local, 1)] = both[None]
    load_far().wait()
    for k in range(half):
        gates_to(far_of(k))
    grecv[pl.ds(sp, 1)] = gsend[pl.ds(sp, 1)]
    for k in range(1, n):
        send_gates(k).start()

    for copy in weights[4:]:
        copy.wait()
    turned = query[...].astype(F32).T
    for q in range(seqs):
        qb[q] = jnp.broadcast_to(turned[:, q : q + 1], (width, width))

    def weigh():
        for k in range(1, n):
            send_gates(k).wait_recv()
        lane = iota((rows, rows), 1)
        line = iota((rows, rows), 0)
        same = (lane // block) == (line // block)
        upto = (same & (line <= lane)).astype(F32)
        whole = same.astype(F32)
        before = (
            (iota((2 * n, 2 * n), 0) // n == iota((2 * n, 2 * n), 1) // n)
            & (iota((2 * n, 2 * n), 1) < iota((2 * n, 2 * n), 0))
        ).astype(F32)
        pre = [
            grecv[:, i, :] + (in_bias if i < 2 else forget_bias)[0:1, i % 2 : i % 2 + 1]
            for i in range(4)
        ]
        forget_pre = jnp.concatenate(pre[2:], axis=0)
        forget = jnp.minimum(forget_pre, 0.0) - jnp.log1p(jnp.exp(-jnp.abs(forget_pre)))
        inside = jnp.dot(forget, upto, preferred_element_type=F32, precision=HIGHEST)
        sums = jnp.dot(forget, whole, preferred_element_type=F32, precision=HIGHEST)
        running = jnp.dot(before, sums, preferred_element_type=F32, precision=HIGHEST) + inside
        totals = [jnp.sum(sums[g * n : (g + 1) * n], axis=0, keepdims=True) for g in range(2)]
        logs = [
            pre[0] + totals[0] - running[:n],
            pre[1] + running[n:] - forget[n:],
        ]
        peak = jnp.concatenate(
            [jnp.maximum(totals[g], jnp.max(logs[g], axis=0, keepdims=True)) for g in range(2)]
            + [jnp.zeros((6, rows), F32)],
            axis=0,
        )
        spot = iota(peak.shape, 1)
        step = 1
        while step < block:
            low, high = pltpu.roll(peak, step, 1), pltpu.roll(peak, rows - step, 1)
            peak = jnp.maximum(peak, jnp.where((spot & step) != 0, low, high))
            step *= 2
        weight = [jnp.exp(logs[g] - peak[g : g + 1]) * width ** (-0.5) for g in range(2)]
        first = side == 0
        parted = [jnp.where(first, w[:half], w[half:]) for w in weight]
        parted += [jnp.where(first, w[half:], w[:half]) for w in weight]
        columns = jnp.concatenate(parted, axis=0).T
        for i in range(4):
            for q in range(seqs):
                for s in range(half):
                    j = i * half + s
                    wb[i, q, s] = jnp.broadcast_to(
                        columns[q * block : (q + 1) * block, j : j + 1], (block, width)
                    )
        own = iota((seqs, rows), 1) // block == iota((seqs, rows), 0)
        return [
            jnp.max(jnp.where(own, peak[g : g + 1], -jnp.inf), axis=1, keepdims=True)
            for g in range(2)
        ]

    def outer(kv, i, q):
        lines = slice(q * block, (q + 1) * block)
        keys = kv[:, lines, :width].reshape(half * block, width)
        values = kv[:, lines, width:].reshape(half * block, width).astype(F32)
        w0 = wb[2 * i, q].reshape(half * block, width)
        w1 = wb[2 * i + 1, q].reshape(half * block, width)
        weighted = jnp.concatenate([values * w0, values * w1], axis=1).astype(BF16)
        keys_f = keys.astype(F32)
        sums = [jnp.sum(keys_f * w, axis=0, keepdims=True) for w in (w0, w1)]
        return tn(keys, weighted), sums

    def project(k):
        source = far_from(k)
        lines = xfar[:, pl.ds(source, 1)].reshape(rows, depth)
        kvf[pl.ds(source, 1)] = jnp.dot(
            lines, wkv[...], preferred_element_type=F32
        ).astype(BF16)[None]

    lag_hand, lag_project = 2, 4
    stable = None
    for step in range(half + lag_project):
        if step < half:
            send_far(step).wait_recv()
            for j in (1, 3, 2):
                spread(j, step).start()
            hand(0, step).start()
        k = step - lag_hand
        if 0 <= k < half:
            for j in (1, 3, 2):
                spread(j, k).wait_recv()
                hand(j, k).start()
        if step == half - 1:
            stable = weigh()
        if step == half:
            for k in range(1, half):
                send_near(k).wait_recv()
            for q in range(seqs):
                acc[q], sums = outer(kvn, 0, q)
                for g in range(2):
                    nrm[g, q : q + 1] = sums[g]
        k = step - lag_project
        if 0 <= k < half:
            for j in range(chips):
                hand(j, k).wait_recv()
            project(k)

    for q in range(seqs):
        more, sums = outer(kvf, 1, q)
        memory = (acc[q] + more).astype(BF16)
        back = memory.astype(F32)
        for g in range(2):
            membuf[g, q, 0] = memory[:, g * width : (g + 1) * width]
            num[g, q : q + 1] = jnp.sum(
                qb[q] * back[:, g * width : (g + 1) * width], axis=0, keepdims=True
            )
            total = nrm[g, q : q + 1] + sums[g]
            nrm[g, q : q + 1] = total
            norm_out[g, q] = total

    hidden = jnp.zeros((seqs, width), F32)
    queries = query[...].astype(F32)
    for g in range(2):
        under = jnp.abs(jnp.sum(queries * nrm[g], axis=1, keepdims=True))
        floor = jnp.maximum(jnp.exp(-stable[g]), 1.0)
        hidden = hidden + num[g] / jnp.maximum(under, floor)
        square = iota((seqs, width), 1) == iota((seqs, width), 0)
        row = jnp.sum(jnp.where(square, stable[g], 0.0), axis=0, keepdims=True)
        stab_out[g] = row[:, :seqs]
    terms = jnp.dot(hidden.astype(BF16), wo[...], preferred_element_type=F32)
    share = terms.shape[1] // tpn
    for t in range(tpn):
        parts[t] = terms[:, t * share : (t + 1) * share]
    for j in range(1, tpn):
        give(j).start()
    for k in range(half):
        send_far(k).wait_send()
        for j in range(1, chips):
            spread(j, k).wait_send()
        for j in range(chips):
            hand(j, k).wait_send()
    for k in range(1, half):
        send_near(k).wait_send()
    for k in range(1, n):
        send_gates(k).wait_send()
    total = parts[tp]
    for j in range(1, tpn):
        give(j).wait()
        total = total + got[j]
    read_out[...] = total.astype(BF16)


def publish(count, *refs):
    sources, targets, sems = refs[:count], refs[count : 2 * count], refs[2 * count]
    copies = [
        pltpu.make_async_copy(a, b, sems.at[i]) for i, (a, b) in enumerate(zip(sources, targets))
    ]
    for copy in copies:
        copy.start()
    for copy in copies:
        copy.wait()


def solution(mesh):
    n, tpn = mesh.shape["sp"], mesh.shape["tp"]

    def body(prompt, w_key, w_value, w_in_gate, w_forget_gate, in_bias, forget_bias, query, w_out):
        depth, heads, width = w_key.shape
        seqs = prompt.shape[0] // n
        block = prompt.shape[1]
        rows = seqs * block
        half = n // 2
        chips = tpn // 2
        wo = w_out.reshape(heads * width, -1)
        columns = wo.shape[1]
        any_ = pl.BlockSpec(memory_space=pl.ANY)
        vmem = pl.BlockSpec(memory_space=pltpu.VMEM)
        dma = pltpu.SemaphoreType.DMA
        shapes = (
            ((2, seqs, heads, width, width), BF16),
            ((2, seqs, heads, width), F32),
            ((2, heads, seqs), F32),
            ((seqs, columns // tpn), BF16),
        )
        held = pl.pallas_call(
            functools.partial(kernel, n, tpn),
            out_shape=tuple(pltpu.VMEM(*shape) for shape in shapes),
            in_specs=[any_] * 9,
            out_specs=(vmem,) * 4,
            scratch_shapes=[
                pltpu.VMEM((n * seqs, block, depth), BF16),
                pltpu.VMEM((depth, 2 * width), BF16),
                pltpu.VMEM((width, columns), BF16),
                pltpu.VMEM((2, depth), BF16),
                pltpu.VMEM((2, depth), BF16),
                pltpu.VMEM((1, 2), F32),
                pltpu.VMEM((1, 2), F32),
                pltpu.VMEM((seqs, width), BF16),
                pltpu.VMEM((16, depth), BF16),
                pltpu.VMEM((half, rows, 2 * width), BF16),
                pltpu.VMEM((half, rows, 2 * width), BF16),
                pltpu.VMEM((half, rows, 2 * width), BF16),
                pltpu.VMEM((n, 8, rows), F32),
                pltpu.VMEM((n, 8, rows), F32),
                pltpu.VMEM((seqs, half, block, depth), BF16),
                pltpu.VMEM((4, seqs, half, block, width), F32),
                pltpu.VMEM((seqs, width, width), F32),
                pltpu.VMEM((seqs, width, 2 * width), F32),
                pltpu.VMEM((2, seqs, width), F32),
                pltpu.VMEM((2, seqs, width), F32),
                pltpu.VMEM((tpn, seqs, columns // tpn), F32),
                pltpu.VMEM((tpn, seqs, columns // tpn), F32),
                dma((8,)),
                dma((half + 1,)),
                dma((half,)),
                dma((half,)),
                dma((half,)),
                dma((half,)),
                dma((n,)),
                dma((n,)),
                dma((chips, half)),
                dma((chips, half)),
                dma((chips, half)),
                dma((chips, half)),
                dma((tpn,)),
                dma((tpn,)),
            ],
            compiler_params=pltpu.CompilerParams(collective_id=0, has_side_effects=True),
            name="memories",
        )(
            prompt, w_key.reshape(depth, width), w_value.reshape(depth, width), wo,
            w_in_gate.reshape(2, depth), w_forget_gate.reshape(2, depth),
            in_bias.reshape(1, 2), forget_bias.reshape(1, 2), query.reshape(seqs, width),
        )
        memory, normal, stable, read = pl.pallas_call(
            functools.partial(publish, len(shapes)),
            out_shape=tuple(jax.ShapeDtypeStruct(*shape) for shape in shapes),
            in_specs=[vmem] * len(shapes),
            out_specs=(any_,) * len(shapes),
            scratch_shapes=[dma((len(shapes),))],
            name="outputs",
        )(*[pltpu.with_memory_space_constraint(a, pltpu.VMEM) for a in held])
        return memory, normal, stable.transpose(0, 2, 1), read

    return jax.shard_map(
        body,
        mesh=mesh,
        in_specs=(
            P("gr", "sp", None),
            P(None, "tp", None),
            P(None, "tp", None),
            P(None, None, "tp"),
            P(None, None, "tp"),
            P(None, "tp"),
            P(None, "tp"),
            P(("gr", "sp"), "tp", None),
            P("tp", None, None),
        ),
        out_specs=(
            P(None, ("gr", "sp"), "tp", None, None),
            P(None, ("gr", "sp"), "tp", None),
            P(None, ("gr", "sp"), "tp"),
            P(("gr", "sp"), "tp"),
        ),
        check_vma=False,
    )
```

time: 87.2 us -> 40.4 us (0.46); the launches traced: 86.2 us -> 40.4 us
  Pallas kernels: 74.9 us -> 39.7 us
  local copies, waits for them, and re-layouts: 10.7 us -> 0 us
    pallas_call x1, Pallas kernels: 74 us -> 38.9 us  [body(): pl.pallas_call(functools.partial(kernel, n, tpn), out_shape=tuple((pltpu....]
    unnamed x5 -> x0, local copies, waits for them, and re-layouts: 8.15 us -> none
    transpose x2 -> x0, local copies, waits for them, and re-layouts: 2.58 us -> none  [the longest x1 1.29 us: body(): w_in_gate.transpose(0, 2, 1)]
where the time goes in v1:
time: 40.4 us
  Pallas kernels  39.7 us (98%)
  between operations  0.64 us (2%)
    pallas_call x1, Pallas kernels, body(): pl.pallas_call(functools.partial(kernel, n, tpn), out_shape=tuple((pltpu....  38.9 us
    pallas_call x1, Pallas kernels, body(): pl.pallas_call(functools.partial(publish, len(shapes)), out_shape=tuple((...  0.84 us

profile of v1, /device:TPU:1, one launch (start us, length us, event | category | flops | bytes accessed | tf_op | source)
XLA Modules:
  0.0 40.4 jit_solution(3040581109072853529)
XLA Ops:
  0.6 38.9 %memories.1 = (bf16[2,8,1,128,128]{4,3,2,1,0:T(8,128)(2,1)S(1)}, f32[2,8,1,128]{3,2,1,0:T(1,128)S(1)}, f32[2,1,8]{2,1,0:T(1,128)S(1)}, bf16[8,128]{1,0:T(8,128)(2,1)S(1)}) custom-call(bf16[128,16,1024]{2,1,0:T(8,128)(2,1)} %prompt.1, bf16[1024,128]{1,0:T(8,128)(2,1)} %bitcast.11, bf16[1024,128]{1,0:T(8,128)(2,1)} %bitcast.12, bf16[128,1024]{1,0:T(8,128)(2,1)} %bitcast.13, ...), custom_call_target="tpu_custom_call" | custom-call | tf_op jit(solution)/shard_map/memories/pallas_call | solution.py:383
  39.5 0.8 %outputs.1 = (bf16[2,8,1,128,128]{4,3,2,1,0:T(8,128)(2,1)}, f32[2,8,1,128]{3,2,1,0:T(1,128)}, f32[2,1,8]{2,1,0:T(1,128)}, bf16[8,128]{1,0:T(8,128)(2,1)}) custom-call(bf16[2,8,1,128,128]{4,3,2,1,0:T(8,128)(2,1)S(1)} %get-tuple-element.12.refs_0_, f32[2,8,1,128]{3,2,1,0:T(1,128)S(1)} %get-tuple-element.13.refs_1_, f32[2,1,8]{2,1,0:T(1,128)S(1)} %get-tuple-element.14.refs_2_, ...), custom_call_target="tpu_custom_call" | custom-call | tf_op jit(solution)/shard_map/outputs/pallas_call | solution.py:433

commit v2 on v1

--- a/solution.py
+++ b/solution.py
@@ -30,19 +30,22 @@
     prompt, wk_hbm, wv_hbm, wo_hbm, ig_hbm, fg_hbm, ib_hbm, fb_hbm, q_hbm,
     membuf, norm_out, stab_out, read_out,
     xall, wkv, wo, in_gate, forget_gate, in_bias, forget_bias, query,
-    wg, kvs, kvn, kvf, gsend, grecv, xfar, wb, qb, acc, num, nrm, parts, got,
-    wsem, lsem, fsend, frecv, nsend, nrecv, gsem, grsem, xsend, xrecv, dsend, drecv, psend, precv,
+    wg, kvs, kvn, kvf, gsend, grecv, xfar, cols, wb, qb, acc, num, nrm, parts, got,
+    lsem, frecv, xrecv, drecv, recv, sent,
 ):
     sp = lax.axis_index("sp")
     tp = lax.axis_index("tp")
     half = n // 2
     cores = 2
     chips = tpn // cores
-    seqs, sources, block, depth = xfar.shape
+    seqs, _, block, depth = xfar.shape
     rows = seqs * block
     width = wo.shape[0]
+    line = half // 2
     side = sp // half
     local = sp - side * half
+    deck, y = local // line, lax.rem(local, line)
+    edge = deck == side
     near_base = side * half
     far_base = half - near_base
     x, c = tp // cores, lax.rem(tp, cores)
@@ -58,44 +61,50 @@
             barrier, inc=1, device_id={"tp": lax.rem(tp + j, tpn)}, device_id_type=MESH
         )
 
-    weights = [
-        pltpu.make_async_copy(wk_hbm, wkv.at[:, :width], wsem.at[0]),
-        pltpu.make_async_copy(wv_hbm, wkv.at[:, width:], wsem.at[1]),
-        pltpu.make_async_copy(ig_hbm, in_gate, wsem.at[2]),
-        pltpu.make_async_copy(fg_hbm, forget_gate, wsem.at[3]),
-        pltpu.make_async_copy(ib_hbm, in_bias, wsem.at[4]),
-        pltpu.make_async_copy(fb_hbm, forget_bias, wsem.at[5]),
-        pltpu.make_async_copy(q_hbm, query, wsem.at[6]),
-        pltpu.make_async_copy(wo_hbm, wo, wsem.at[7]),
+    def far_from(k):
+        deck_of = side if k < line else 1 - side
+        return deck_of * line + lax.rem(y + line - k % line, line)
+
+    def far_to(i):
+        deck_of = 1 - side if i % 2 else side
+        return far_base + deck_of * line + lax.rem(y + i // 2, line)
+
+    def near_to(k):
+        deck_of = 1 - deck if k < line else deck
+        turn = k if k < line else k + 1
+        return near_base + deck_of * line + lax.rem(y + turn, line)
+
+    def load(i):
+        base = near_base if i == 0 else far_base
+        part = pl.ds(base * seqs, half * seqs)
+        return pltpu.make_async_copy(prompt.at[part], xall.at[part], lsem.at[i])
+
+    gate_loads = [
+        pltpu.make_async_copy(ig_hbm, in_gate, lsem.at[2]),
+        pltpu.make_async_copy(fg_hbm, forget_gate, lsem.at[3]),
     ]
-
-    def near_of(k):
-        return near_base + lax.rem(local + k, half)
-
-    def far_of(k):
-        return far_base + lax.rem(local + k, half)
-
-    def far_from(k):
-        return lax.rem(local + half - k, half)
-
-    def load(k):
-        return pltpu.make_async_copy(
-            prompt.at[pl.ds(near_of(k) * seqs, seqs)],
-            xall.at[pl.ds(near_of(k) * seqs, seqs)],
-            lsem.at[k],
-        )
-
-    def load_far():
-        part = pl.ds(far_base * seqs, half * seqs)
-        return pltpu.make_async_copy(prompt.at[part], xall.at[part], lsem.at[half])
-
-    def send_far(k):
-        dest = far_of(k)
+    weight_loads = [
+        pltpu.make_async_copy(wk_hbm, wkv.at[:, :width], lsem.at[4]),
+        pltpu.make_async_copy(wv_hbm, wkv.at[:, width:], lsem.at[5]),
+    ]
+    late_loads = [
+        pltpu.make_async_copy(ib_hbm, in_bias, lsem.at[6]),
+        pltpu.make_async_copy(fb_hbm, forget_bias, lsem.at[7]),
+        pltpu.make_async_copy(q_hbm, query, lsem.at[8]),
+        pltpu.make_async_copy(wo_hbm, wo, lsem.at[9]),
+    ]
+
+    def arrived(ref, sem):
+        pltpu.make_async_copy(ref, ref, sem).wait()
+
+    def send_far(i):
+        dest = far_to(i)
+        deck_of = jnp.where(edge, 1, 0)
         return pltpu.make_async_remote_copy(
             src_ref=prompt.at[dest * seqs + tp],
             dst_ref=xfar.at[tp, local],
-            send_sem=fsend.at[k],
-            recv_sem=frecv.at[k],
+            send_sem=sent.at[0],
+            recv_sem=frecv.at[deck_of * line + i // 2],
             device_id={"sp": dest},
             device_id_type=MESH,
         )
@@ -104,9 +113,9 @@
         return pltpu.make_async_remote_copy(
             src_ref=kvs.at[k],
             dst_ref=kvn.at[local],
-            send_sem=nsend.at[k],
-            recv_sem=nrecv.at[k],
-            device_id={"sp": near_of(k)},
+            send_sem=sent.at[1],
+            recv_sem=recv.at[0],
+            device_id={"sp": near_to(k)},
             device_id_type=MESH,
         )
 
@@ -115,8 +124,8 @@
         return pltpu.make_async_remote_copy(
             src_ref=gsend.at[dest],
             dst_ref=grecv.at[sp],
-            send_sem=gsem.at[k],
-            recv_sem=grsem.at[k],
+            send_sem=sent.at[2],
+            recv_sem=recv.at[1],
             device_id={"sp": dest},
             device_id_type=MESH,
         )
@@ -126,7 +135,7 @@
         return pltpu.make_async_remote_copy(
             src_ref=piece,
             dst_ref=piece,
-            send_sem=xsend.at[j, k],
+            send_sem=sent.at[3],
             recv_sem=xrecv.at[j, k],
             device_id={"tp": lax.rem(x + j, chips) * cores + c},
             device_id_type=MESH,
@@ -138,8 +147,8 @@
         return pltpu.make_async_remote_copy(
             src_ref=piece,
             dst_ref=piece,
-            send_sem=dsend.at[j, k],
-            recv_sem=drecv.at[j, k],
+            send_sem=sent.at[4],
+            recv_sem=drecv.at[k],
             device_id={"tp": partner},
             device_id_type=MESH,
         )
@@ -149,25 +158,22 @@
         return pltpu.make_async_remote_copy(
             src_ref=parts.at[peer],
             dst_ref=got.at[j],
-            send_sem=psend.at[j],
-            recv_sem=precv.at[j],
+            send_sem=sent.at[5],
+            recv_sem=recv.at[2],
             device_id={"tp": peer},
             device_id_type=MESH,
         )
 
-    for copy in weights[:4]:
+    for copy in gate_loads:
         copy.start()
-    for k in list(range(1, half)) + [0]:
-        load(k).start()
-    load_far().start()
-    for copy in weights[4:]:
+    load(0).start()
+    load(1).start()
+    for copy in weight_loads + late_loads:
         copy.start()
-    pl.semaphore_wait(barrier, n - 1 + tpn - 1)
-    for k in range(half):
-        send_far(k).start()
-
-    for copy in weights[:4]:
+
+    for copy in gate_loads:
         copy.wait()
+    load(0).wait()
     wg[...] = jnp.concatenate(
         [in_gate[...].astype(F32), forget_gate[...].astype(F32), jnp.zeros((wg.shape[0] - 4, depth), F32)],
         axis=0,
@@ -176,39 +182,44 @@
     def rows_of(dest):
         return xall[pl.ds(dest * seqs, seqs)].reshape(rows, depth)
 
-    def gates_to(dest):
-        gsend[pl.ds(dest, 1)] = nt(wg[...], rows_of(dest))[: gsend.shape[1]][None]
-
-    for k in list(range(1, half)) + [0]:
-        load(k).wait()
-        dest = near_of(k)
+    for base in (near_base, far_base):
+        if base is far_base:
+            load(1).wait()
+        for k in range(half):
+            gsend[pl.ds(base + k, 1)] = nt(wg[...], rows_of(base + k))[:4][None]
+    grecv[pl.ds(sp, 1)] = gsend[pl.ds(sp, 1)]
+    pl.semaphore_wait(barrier, n - 1 + tpn - 1)
+    for k in range(1, n):
+        send_gates(k).start()
+
+    @pl.when(jnp.logical_not(edge))
+    def _():
+        for i in range(half):
+            send_far(i).start()
+
+    for copy in weight_loads:
+        copy.wait()
+    for k in range(half):
+        dest = near_to(k)
         both = jnp.dot(rows_of(dest), wkv[...], preferred_element_type=F32).astype(BF16)
-        gates_to(dest)
-        if k:
+        if k < half - 1:
             kvs[k] = both
             send_near(k).start()
         else:
             kvn[pl.ds(local, 1)] = both[None]
-    load_far().wait()
-    for k in range(half):
-        gates_to(far_of(k))
-    grecv[pl.ds(sp, 1)] = gsend[pl.ds(sp, 1)]
-    for k in range(1, n):
-        send_gates(k).start()
-
-    for copy in weights[4:]:
-        copy.wait()
-    turned = query[...].astype(F32).T
-    for q in range(seqs):
-        qb[q] = jnp.broadcast_to(turned[:, q : q + 1], (width, width))
+        if k == line - 1:
+
+            @pl.when(edge)
+            def _():
+                for i in range(half):
+                    send_far(i).start()
+
 
     def weigh():
-        for k in range(1, n):
-            send_gates(k).wait_recv()
         lane = iota((rows, rows), 1)
-        line = iota((rows, rows), 0)
-        same = (lane // block) == (line // block)
-        upto = (same & (line <= lane)).astype(F32)
+        down = iota((rows, rows), 0)
+        same = (lane // block) == (down // block)
+        upto = (same & (down <= lane)).astype(F32)
         whole = same.astype(F32)
         before = (
             (iota((2 * n, 2 * n), 0) // n == iota((2 * n, 2 * n), 1) // n)
@@ -243,19 +254,20 @@
         first = side == 0
         parted = [jnp.where(first, w[:half], w[half:]) for w in weight]
         parted += [jnp.where(first, w[half:], w[:half]) for w in weight]
-        columns = jnp.concatenate(parted, axis=0).T
-        for i in range(4):
-            for q in range(seqs):
-                for s in range(half):
-                    j = i * half + s
-                    wb[i, q, s] = jnp.broadcast_to(
-                        columns[q * block : (q + 1) * block, j : j + 1], (block, width)
-                    )
+        cols[...] = jnp.concatenate(parted, axis=0).T
         own = iota((seqs, rows), 1) // block == iota((seqs, rows), 0)
         return [
             jnp.max(jnp.where(own, peak[g : g + 1], -jnp.inf), axis=1, keepdims=True)
             for g in range(2)
         ]
+
+    def widen(i):
+        for q in range(seqs):
+            for s in range(half):
+                j = i * half + s
+                wb[i, q, s] = jnp.broadcast_to(
+                    cols[q * block : (q + 1) * block, j : j + 1], (block, width)
+                )
 
     def outer(kv, i, q):
         lines = slice(q * block, (q + 1) * block)
@@ -279,28 +291,36 @@
     stable = None
     for step in range(half + lag_project):
         if step < half:
-            send_far(step).wait_recv()
-            for j in (1, 3, 2):
+            arrived(xfar.at[0, 0], frecv.at[step])
+            for j in (2, 1, 3):
                 spread(j, step).start()
             hand(0, step).start()
         k = step - lag_hand
         if 0 <= k < half:
             for j in (1, 3, 2):
-                spread(j, k).wait_recv()
+                arrived(xfar.at[0, 0], xrecv.at[j, k])
                 hand(j, k).start()
-        if step == half - 1:
+        if step == 0:
+            for copy in late_loads:
+                copy.wait()
+            turned = query[...].astype(F32).T
+            for q in range(seqs):
+                qb[q] = jnp.broadcast_to(turned[:, q : q + 1], (width, width))
+        if step == 2:
+            arrived(grecv.at[pl.ds(0, n - 1)], recv.at[1])
             stable = weigh()
+        if step in (3, 4):
+            widen(2 * (step - 3))
+            widen(2 * (step - 3) + 1)
         if step == half:
-            for k in range(1, half):
-                send_near(k).wait_recv()
+            arrived(kvn.at[pl.ds(0, half - 1)], recv.at[0])
             for q in range(seqs):
                 acc[q], sums = outer(kvn, 0, q)
                 for g in range(2):
                     nrm[g, q : q + 1] = sums[g]
         k = step - lag_project
         if 0 <= k < half:
-            for j in range(chips):
-                hand(j, k).wait_recv()
+            arrived(xfar.at[0, pl.ds(0, chips)], drecv.at[k])
             project(k)
 
     for q in range(seqs):
@@ -331,19 +351,15 @@
         parts[t] = terms[:, t * share : (t + 1) * share]
     for j in range(1, tpn):
         give(j).start()
-    for k in range(half):
-        send_far(k).wait_send()
-        for j in range(1, chips):
-            spread(j, k).wait_send()
-        for j in range(chips):
-            hand(j, k).wait_send()
-    for k in range(1, half):
-        send_near(k).wait_send()
-    for k in range(1, n):
-        send_gates(k).wait_send()
+    arrived(xfar.at[0], sent.at[0])
+    arrived(kvn.at[pl.ds(0, half - 1)], sent.at[1])
+    arrived(grecv.at[pl.ds(0, n - 1)], sent.at[2])
+    arrived(xfar.at[pl.ds(0, chips - 1)], sent.at[3])
+    arrived(xfar.at[pl.ds(0, chips)], sent.at[4])
+    arrived(got.at[pl.ds(0, tpn - 1)], sent.at[5])
+    arrived(got.at[pl.ds(0, tpn - 1)], recv.at[2])
     total = parts[tp]
     for j in range(1, tpn):
-        give(j).wait()
         total = total + got[j]
     read_out[...] = total.astype(BF16)
 
@@ -398,9 +414,10 @@
                 pltpu.VMEM((half, rows, 2 * width), BF16),
                 pltpu.VMEM((half, rows, 2 * width), BF16),
                 pltpu.VMEM((half, rows, 2 * width), BF16),
-                pltpu.VMEM((n, 8, rows), F32),
-                pltpu.VMEM((n, 8, rows), F32),
+                pltpu.VMEM((n, 4, rows), F32),
+                pltpu.VMEM((n, 4, rows), F32),
                 pltpu.VMEM((seqs, half, block, depth), BF16),
+                pltpu.VMEM((rows, 4 * half), F32),
                 pltpu.VMEM((4, seqs, half, block, width), F32),
                 pltpu.VMEM((seqs, width, width), F32),
                 pltpu.VMEM((seqs, width, 2 * width), F32),
@@ -408,20 +425,12 @@
                 pltpu.VMEM((2, seqs, width), F32),
                 pltpu.VMEM((tpn, seqs, columns // tpn), F32),
                 pltpu.VMEM((tpn, seqs, columns // tpn), F32),
-                dma((8,)),
-                dma((half + 1,)),
+                dma((10,)),
                 dma((half,)),
+                dma((chips, half)),
                 dma((half,)),
-                dma((half,)),
-                dma((half,)),
-                dma((n,)),
-                dma((n,)),
-                dma((chips, half)),
-                dma((chips, half)),
-                dma((chips, half)),
-                dma((chips, half)),
-                dma((tpn,)),
-                dma((tpn,)),
+                dma((3,)),
+                dma((6,)),
             ],
             compiler_params=pltpu.CompilerParams(collective_id=0, has_side_effects=True),
             name="memories",

time: 40.4 us -> 36.8 us (0.911)
  Pallas kernels: 39.7 us -> 36.1 us
    pallas_call x1, Pallas kernels: 38.9 us -> 35.2 us  [body(): pl.pallas_call(functools.partial(kernel, n, tpn), out_shape=tuple((pltpu....]
where the time goes in v2:
time: 36.8 us; the launch traced here: 36.7 us
  Pallas kernels  36.1 us (98%)
  between operations  0.64 us (2%)
    pallas_call x1, Pallas kernels, body(): pl.pallas_call(functools.partial(kernel, n, tpn), out_shape=tuple((pltpu....  35.2 us
    pallas_call x1, Pallas kernels, body(): pl.pallas_call(functools.partial(publish, len(shapes)), out_shape=tuple((...  0.84 us

profile of v2, /device:TPU:1, one launch (start us, length us, event | category | flops | bytes accessed | tf_op | source)
XLA Modules:
  0.0 36.7 jit_solution(14908959724257697163)
XLA Ops:
  0.6 35.2 %memories.1 = (bf16[2,8,1,128,128]{4,3,2,1,0:T(8,128)(2,1)S(1)}, f32[2,8,1,128]{3,2,1,0:T(1,128)S(1)}, f32[2,1,8]{2,1,0:T(1,128)S(1)}, bf16[8,128]{1,0:T(8,128)(2,1)S(1)}) custom-call(bf16[128,16,1024]{2,1,0:T(8,128)(2,1)} %prompt.1, bf16[1024,128]{1,0:T(8,128)(2,1)} %bitcast.11, bf16[1024,128]{1,0:T(8,128)(2,1)} %bitcast.12, bf16[128,1024]{1,0:T(8,128)(2,1)} %bitcast.13, ...), custom_call_target="tpu_custom_call" | custom-call | tf_op jit(solution)/shard_map/memories/pallas_call | solution.py:399
  35.9 0.8 %outputs.1 = (bf16[2,8,1,128,128]{4,3,2,1,0:T(8,128)(2,1)}, f32[2,8,1,128]{3,2,1,0:T(1,128)}, f32[2,1,8]{2,1,0:T(1,128)}, bf16[8,128]{1,0:T(8,128)(2,1)}) custom-call(bf16[2,8,1,128,128]{4,3,2,1,0:T(8,128)(2,1)S(1)} %get-tuple-element.12.refs_0_, f32[2,8,1,128]{3,2,1,0:T(1,128)S(1)} %get-tuple-element.13.refs_1_, f32[2,1,8]{2,1,0:T(1,128)S(1)} %get-tuple-element.14.refs_2_, ...), custom_call_target="tpu_custom_call" | custom-call | tf_op jit(solution)/shard_map/outputs/pallas_call | solution.py:442

commit v3 on v2

--- a/solution.py
+++ b/solution.py
@@ -23,6 +23,9 @@
 
 def iota(shape, axis):
     return lax.broadcasted_iota(jnp.int32, shape, axis)
+
+
+NEAR_ORDER = (0, 1, 4, "far", 2, 5, 3, 6)
 
 
 def kernel(
@@ -61,37 +64,42 @@
             barrier, inc=1, device_id={"tp": lax.rem(tp + j, tpn)}, device_id_type=MESH
         )
 
+    turns = line - 1
+    steps = 2 * turns
+
     def far_from(k):
-        deck_of = side if k < line else 1 - side
-        return deck_of * line + lax.rem(y + line - k % line, line)
+        deck_of = 1 - side if k < turns else side
+        return deck_of * line + lax.rem(y + line - 1 - k % turns, line)
 
     def far_to(i):
         deck_of = 1 - side if i % 2 else side
-        return far_base + deck_of * line + lax.rem(y + i // 2, line)
+        return far_base + deck_of * line + lax.rem(y + 1 + i // 2, line)
 
     def near_to(k):
         deck_of = 1 - deck if k < line else deck
         turn = k if k < line else k + 1
         return near_base + deck_of * line + lax.rem(y + turn, line)
 
+    pieces = 4
+
     def load(i):
-        base = near_base if i == 0 else far_base
-        part = pl.ds(base * seqs, half * seqs)
+        base = (near_base if i < pieces // 2 else far_base) + i % (pieces // 2) * (2 * half // pieces)
+        part = pl.ds(base * seqs, 2 * half // pieces * seqs)
         return pltpu.make_async_copy(prompt.at[part], xall.at[part], lsem.at[i])
 
     gate_loads = [
-        pltpu.make_async_copy(ig_hbm, in_gate, lsem.at[2]),
-        pltpu.make_async_copy(fg_hbm, forget_gate, lsem.at[3]),
+        pltpu.make_async_copy(ig_hbm, in_gate, lsem.at[4]),
+        pltpu.make_async_copy(fg_hbm, forget_gate, lsem.at[5]),
     ]
     weight_loads = [
-        pltpu.make_async_copy(wk_hbm, wkv.at[:, :width], lsem.at[4]),
-        pltpu.make_async_copy(wv_hbm, wkv.at[:, width:], lsem.at[5]),
+        pltpu.make_async_copy(wk_hbm, wkv.at[:, :width], lsem.at[6]),
+        pltpu.make_async_copy(wv_hbm, wkv.at[:, width:], lsem.at[7]),
     ]
     late_loads = [
-        pltpu.make_async_copy(ib_hbm, in_bias, lsem.at[6]),
-        pltpu.make_async_copy(fb_hbm, forget_bias, lsem.at[7]),
-        pltpu.make_async_copy(q_hbm, query, lsem.at[8]),
-        pltpu.make_async_copy(wo_hbm, wo, lsem.at[9]),
+        pltpu.make_async_copy(ib_hbm, in_bias, lsem.at[8]),
+        pltpu.make_async_copy(fb_hbm, forget_bias, lsem.at[9]),
+        pltpu.make_async_copy(q_hbm, query, lsem.at[10]),
+        pltpu.make_async_copy(wo_hbm, wo, lsem.at[11]),
     ]
 
     def arrived(ref, sem):
@@ -99,12 +107,12 @@
 
     def send_far(i):
         dest = far_to(i)
-        deck_of = jnp.where(edge, 1, 0)
+        late = jnp.where(edge, 0, turns)
         return pltpu.make_async_remote_copy(
             src_ref=prompt.at[dest * seqs + tp],
             dst_ref=xfar.at[tp, local],
             send_sem=sent.at[0],
-            recv_sem=frecv.at[deck_of * line + i // 2],
+            recv_sem=frecv.at[late + i // 2],
             device_id={"sp": dest},
             device_id_type=MESH,
         )
@@ -119,6 +127,16 @@
             device_id_type=MESH,
         )
 
+    def send_line(i):
+        return pltpu.make_async_remote_copy(
+            src_ref=kvs.at[half - 1 + i],
+            dst_ref=kvf.at[local],
+            send_sem=sent.at[1],
+            recv_sem=recv.at[3],
+            device_id={"sp": far_base + i * line + y},
+            device_id_type=MESH,
+        )
+
     def send_gates(k):
         dest = lax.rem(sp + k, n)
         return pltpu.make_async_remote_copy(
@@ -166,14 +184,13 @@
 
     for copy in gate_loads:
         copy.start()
-    load(0).start()
-    load(1).start()
+    for i in range(pieces):
+        load(i).start()
     for copy in weight_loads + late_loads:
         copy.start()
 
     for copy in gate_loads:
         copy.wait()
-    load(0).wait()
     wg[...] = jnp.concatenate(
         [in_gate[...].astype(F32), forget_gate[...].astype(F32), jnp.zeros((wg.shape[0] - 4, depth), F32)],
         axis=0,
@@ -182,38 +199,47 @@
     def rows_of(dest):
         return xall[pl.ds(dest * seqs, seqs)].reshape(rows, depth)
 
-    for base in (near_base, far_base):
-        if base is far_base:
-            load(1).wait()
-        for k in range(half):
-            gsend[pl.ds(base + k, 1)] = nt(wg[...], rows_of(base + k))[:4][None]
+    def gates(start, stop):
+        for i in range(start, stop):
+            if i % (2 * half // pieces) == 0:
+                load(i // (2 * half // pieces)).wait()
+            dest = (near_base if i < half else far_base) + i % half
+            gsend[pl.ds(dest, 1)] = nt(wg[...], rows_of(dest))[:4][None]
+
+    gates(0, half)
+    pl.semaphore_wait(barrier, n - 1 + tpn - 1)
+    inner = jnp.logical_not(edge)
+
+    @pl.when(edge)
+    def _():
+        for i in range(steps):
+            send_far(i).start()
+
+    gates(half, 2 * half)
     grecv[pl.ds(sp, 1)] = gsend[pl.ds(sp, 1)]
-    pl.semaphore_wait(barrier, n - 1 + tpn - 1)
     for k in range(1, n):
         send_gates(k).start()
-
-    @pl.when(jnp.logical_not(edge))
-    def _():
-        for i in range(half):
-            send_far(i).start()
-
     for copy in weight_loads:
         copy.wait()
-    for k in range(half):
-        dest = near_to(k)
-        both = jnp.dot(rows_of(dest), wkv[...], preferred_element_type=F32).astype(BF16)
-        if k < half - 1:
-            kvs[k] = both
-            send_near(k).start()
-        else:
-            kvn[pl.ds(local, 1)] = both[None]
-        if k == line - 1:
-
-            @pl.when(edge)
+
+    def keys_values(dest):
+        return jnp.dot(rows_of(dest), wkv[...], preferred_element_type=F32).astype(BF16)
+
+    for k in NEAR_ORDER:
+        if k == "far":
+
+            @pl.when(inner)
             def _():
-                for i in range(half):
+                for i in range(steps):
                     send_far(i).start()
 
+            continue
+        kvs[k] = keys_values(near_to(k))
+        send_near(k).start()
+    for i in range(2):
+        kvs[half - 1 + i] = keys_values(far_base + i * line + y)
+        send_line(i).start()
+    kvn[pl.ds(local, 1)] = keys_values(near_to(half - 1))[None]
 
     def weigh():
         lane = iota((rows, rows), 1)
@@ -280,49 +306,59 @@
         sums = [jnp.sum(keys_f * w, axis=0, keepdims=True) for w in (w0, w1)]
         return tn(keys, weighted), sums
 
-    def project(k):
-        source = far_from(k)
-        lines = xfar[:, pl.ds(source, 1)].reshape(rows, depth)
-        kvf[pl.ds(source, 1)] = jnp.dot(
-            lines, wkv[...], preferred_element_type=F32
-        ).astype(BF16)[None]
-
-    lag_hand, lag_project = 2, 4
-    stable = None
-    for step in range(half + lag_project):
-        if step < half:
-            arrived(xfar.at[0, 0], frecv.at[step])
+    def project(p):
+        found = [far_from(2 * p), far_from(2 * p + 1)]
+        lines = [xfar[:, pl.ds(source, 1)].reshape(rows, depth) for source in found]
+        both = jnp.dot(
+            jnp.concatenate(lines, axis=0), wkv[...], preferred_element_type=F32
+        ).astype(BF16)
+        for i, source in enumerate(found):
+            kvf[pl.ds(source, 1)] = both[i * rows : (i + 1) * rows][None]
+
+    def own(p):
+        for k in (2 * p, 2 * p + 1):
+            arrived(xfar.at[0, 0], frecv.at[k])
             for j in (2, 1, 3):
-                spread(j, step).start()
-            hand(0, step).start()
-        k = step - lag_hand
-        if 0 <= k < half:
+                spread(j, k).start()
+            hand(0, k).start()
+
+    def pass_on(p):
+        for k in (2 * p, 2 * p + 1):
             for j in (1, 3, 2):
                 arrived(xfar.at[0, 0], xrecv.at[j, k])
                 hand(j, k).start()
-        if step == 0:
-            for copy in late_loads:
-                copy.wait()
-            turned = query[...].astype(F32).T
-            for q in range(seqs):
-                qb[q] = jnp.broadcast_to(turned[:, q : q + 1], (width, width))
-        if step == 2:
-            arrived(grecv.at[pl.ds(0, n - 1)], recv.at[1])
-            stable = weigh()
-        if step in (3, 4):
-            widen(2 * (step - 3))
-            widen(2 * (step - 3) + 1)
-        if step == half:
-            arrived(kvn.at[pl.ds(0, half - 1)], recv.at[0])
-            for q in range(seqs):
-                acc[q], sums = outer(kvn, 0, q)
-                for g in range(2):
-                    nrm[g, q : q + 1] = sums[g]
-        k = step - lag_project
-        if 0 <= k < half:
+
+    def collect(p):
+        for k in (2 * p, 2 * p + 1):
             arrived(xfar.at[0, pl.ds(0, chips)], drecv.at[k])
-            project(k)
-
+        project(p)
+
+    own(0)
+    for copy in late_loads:
+        copy.wait()
+    turned = query[...].astype(F32).T
+    for q in range(seqs):
+        qb[q] = jnp.broadcast_to(turned[:, q : q + 1], (width, width))
+    arrived(grecv.at[pl.ds(0, n - 1)], recv.at[1])
+    stable = weigh()
+    own(1)
+    widen(0)
+    widen(1)
+    pass_on(0)
+    own(2)
+    widen(2)
+    widen(3)
+    pass_on(1)
+    collect(0)
+    pass_on(2)
+    arrived(kvn.at[pl.ds(0, half - 1)], recv.at[0])
+    for q in range(seqs):
+        acc[q], sums = outer(kvn, 0, q)
+        for g in range(2):
+            nrm[g, q : q + 1] = sums[g]
+    collect(1)
+    collect(2)
+    arrived(kvf.at[pl.ds(0, 2)], recv.at[3])
     for q in range(seqs):
         more, sums = outer(kvf, 1, q)
         memory = (acc[q] + more).astype(BF16)
@@ -351,11 +387,11 @@
         parts[t] = terms[:, t * share : (t + 1) * share]
     for j in range(1, tpn):
         give(j).start()
-    arrived(xfar.at[0], sent.at[0])
-    arrived(kvn.at[pl.ds(0, half - 1)], sent.at[1])
+    arrived(xfar.at[0, pl.ds(0, steps)], sent.at[0])
+    arrived(kvs, sent.at[1])
     arrived(grecv.at[pl.ds(0, n - 1)], sent.at[2])
-    arrived(xfar.at[pl.ds(0, chips - 1)], sent.at[3])
-    arrived(xfar.at[pl.ds(0, chips)], sent.at[4])
+    arrived(xfar.at[pl.ds(0, chips - 1), pl.ds(0, steps)], sent.at[3])
+    arrived(xfar.at[pl.ds(0, chips), pl.ds(0, steps)], sent.at[4])
     arrived(got.at[pl.ds(0, tpn - 1)], sent.at[5])
     arrived(got.at[pl.ds(0, tpn - 1)], recv.at[2])
     total = parts[tp]
@@ -385,6 +421,7 @@
         rows = seqs * block
         half = n // 2
         chips = tpn // 2
+        steps = 2 * (half // 2 - 1)
         wo = w_out.reshape(heads * width, -1)
         columns = wo.shape[1]
         any_ = pl.BlockSpec(memory_space=pl.ANY)
@@ -411,7 +448,7 @@
                 pltpu.VMEM((1, 2), F32),
                 pltpu.VMEM((seqs, width), BF16),
                 pltpu.VMEM((16, depth), BF16),
-                pltpu.VMEM((half, rows, 2 * width), BF16),
+                pltpu.VMEM((half + 1, rows, 2 * width), BF16),
                 pltpu.VMEM((half, rows, 2 * width), BF16),
                 pltpu.VMEM((half, rows, 2 * width), BF16),
                 pltpu.VMEM((n, 4, rows), F32),
@@ -425,11 +462,11 @@
                 pltpu.VMEM((2, seqs, width), F32),
                 pltpu.VMEM((tpn, seqs, columns // tpn), F32),
                 pltpu.VMEM((tpn, seqs, columns // tpn), F32),
-                dma((10,)),
-                dma((half,)),
-                dma((chips, half)),
-                dma((half,)),
-                dma((3,)),
+                dma((12,)),
+                dma((steps,)),
+                dma((chips, steps)),
+                dma((steps,)),
+                dma((4,)),
                 dma((6,)),
             ],
             compiler_params=pltpu.CompilerParams(collective_id=0, has_side_effects=True),

time: 36.8 us -> 33.2 us (0.902)
  Pallas kernels: 36.1 us -> 32.4 us
    pallas_call x1, Pallas kernels: 35.2 us -> 31.6 us  [body(): pl.pallas_call(functools.partial(kernel, n, tpn), out_shape=tuple((pltpu....]
where the time goes in v3:
time: 33.2 us; the launch traced here: 33.1 us
  Pallas kernels  32.4 us (98%)
  between operations  0.64 us (2%)
    pallas_call x1, Pallas kernels, body(): pl.pallas_call(functools.partial(kernel, n, tpn), out_shape=tuple((pltpu....  31.6 us
    pallas_call x1, Pallas kernels, body(): pl.pallas_call(functools.partial(publish, len(shapes)), out_shape=tuple((...  0.84 us

profile of v3, /device:TPU:1, one launch (start us, length us, event | category | flops | bytes accessed | tf_op | source)
XLA Modules:
  0.0 33.1 jit_solution(421284525635293394)
XLA Ops:
  0.6 31.6 %memories.1 = (bf16[2,8,1,128,128]{4,3,2,1,0:T(8,128)(2,1)S(1)}, f32[2,8,1,128]{3,2,1,0:T(1,128)S(1)}, f32[2,1,8]{2,1,0:T(1,128)S(1)}, bf16[8,128]{1,0:T(8,128)(2,1)S(1)}) custom-call(bf16[128,16,1024]{2,1,0:T(8,128)(2,1)} %prompt.1, bf16[1024,128]{1,0:T(8,128)(2,1)} %bitcast.11, bf16[1024,128]{1,0:T(8,128)(2,1)} %bitcast.12, bf16[128,1024]{1,0:T(8,128)(2,1)} %bitcast.13, ...), custom_call_target="tpu_custom_call" | custom-call | tf_op jit(solution)/shard_map/memories/pallas_call | solution.py:436
  32.2 0.8 %outputs.1 = (bf16[2,8,1,128,128]{4,3,2,1,0:T(8,128)(2,1)}, f32[2,8,1,128]{3,2,1,0:T(1,128)}, f32[2,1,8]{2,1,0:T(1,128)}, bf16[8,128]{1,0:T(8,128)(2,1)}) custom-call(bf16[2,8,1,128,128]{4,3,2,1,0:T(8,128)(2,1)S(1)} %get-tuple-element.12.refs_0_, f32[2,8,1,128]{3,2,1,0:T(1,128)S(1)} %get-tuple-element.13.refs_1_, f32[2,1,8]{2,1,0:T(1,128)S(1)} %get-tuple-element.14.refs_2_, ...), custom_call_target="tpu_custom_call" | custom-call | tf_op jit(solution)/shard_map/outputs/pallas_call | solution.py:479

commit v4 on v3

--- a/solution.py
+++ b/solution.py
@@ -25,14 +25,38 @@
     return lax.broadcasted_iota(jnp.int32, shape, axis)
 
 
-NEAR_ORDER = (0, 1, 4, "far", 2, 5, 3, 6)
+NEAR_ORDER = ("far", 0, 1, 4, 2, 5, 3, 6)
+ORDER = (
+    ("own", 0),
+    ("own", 1),
+    ("queries", 0),
+    ("own", 2),
+    ("own", 3),
+    ("pass", 0),
+    ("own", 4),
+    ("own", 5),
+    ("pass", 1),
+    ("gates", 0),
+    ("pass", 2),
+    ("widen", 0),
+    ("widen", 1),
+    ("pass", 3),
+    ("widen", 2),
+    ("widen", 3),
+    ("collect", 0),
+    ("near", 0),
+    ("pass", 4),
+    ("collect", 1),
+    ("pass", 5),
+    ("collect", 2),
+)
 
 
 def kernel(
     n, tpn,
     prompt, wk_hbm, wv_hbm, wo_hbm, ig_hbm, fg_hbm, ib_hbm, fb_hbm, q_hbm,
     membuf, norm_out, stab_out, read_out,
-    xall, wkv, wo, in_gate, forget_gate, in_bias, forget_bias, query,
+    xall, wkv, wo, gate_w, biases, query,
     wg, kvs, kvn, kvf, gsend, grecv, xfar, cols, wb, qb, acc, num, nrm, parts, got,
     lsem, frecv, xrecv, drecv, recv, sent,
 ):
@@ -55,9 +79,19 @@
     partner = x * cores + 1 - c
 
     barrier = pltpu.get_barrier_semaphore()
-    for k in range(1, n):
+    for i in range(half):
         pl.semaphore_signal(
-            barrier, inc=1, device_id={"sp": lax.rem(sp + k, n)}, device_id_type=MESH
+            barrier,
+            inc=1,
+            device_id={"sp": far_base + lax.rem(local + half // 2 + i, half)},
+            device_id_type=MESH,
+        )
+    for k in range(1, half):
+        pl.semaphore_signal(
+            barrier,
+            inc=1,
+            device_id={"sp": near_base + lax.rem(local + k, half)},
+            device_id_type=MESH,
         )
     for j in range(1, tpn):
         pl.semaphore_signal(
@@ -67,13 +101,16 @@
     turns = line - 1
     steps = 2 * turns
 
+    def turn_of(i):
+        return (line // 2, 1, line - 1)[i]
+
     def far_from(k):
         deck_of = 1 - side if k < turns else side
-        return deck_of * line + lax.rem(y + line - 1 - k % turns, line)
+        return deck_of * line + lax.rem(y + line - turn_of(k % turns), line)
 
     def far_to(i):
-        deck_of = 1 - side if i % 2 else side
-        return far_base + deck_of * line + lax.rem(y + 1 + i // 2, line)
+        deck_of = 1 - side if i < turns else side
+        return far_base + deck_of * line + lax.rem(y + turn_of(i % turns), line)
 
     def near_to(k):
         deck_of = 1 - deck if k < line else deck
@@ -88,18 +125,18 @@
         return pltpu.make_async_copy(prompt.at[part], xall.at[part], lsem.at[i])
 
     gate_loads = [
-        pltpu.make_async_copy(ig_hbm, in_gate, lsem.at[4]),
-        pltpu.make_async_copy(fg_hbm, forget_gate, lsem.at[5]),
+        pltpu.make_async_copy(ig_hbm, gate_w.at[0], lsem.at[4]),
+        pltpu.make_async_copy(fg_hbm, gate_w.at[1], lsem.at[4]),
     ]
     weight_loads = [
-        pltpu.make_async_copy(wk_hbm, wkv.at[:, :width], lsem.at[6]),
-        pltpu.make_async_copy(wv_hbm, wkv.at[:, width:], lsem.at[7]),
+        pltpu.make_async_copy(wk_hbm, wkv.at[:, :width], lsem.at[5]),
+        pltpu.make_async_copy(wv_hbm, wkv.at[:, width:], lsem.at[5]),
     ]
     late_loads = [
-        pltpu.make_async_copy(ib_hbm, in_bias, lsem.at[8]),
-        pltpu.make_async_copy(fb_hbm, forget_bias, lsem.at[9]),
-        pltpu.make_async_copy(q_hbm, query, lsem.at[10]),
-        pltpu.make_async_copy(wo_hbm, wo, lsem.at[11]),
+        pltpu.make_async_copy(ib_hbm, biases.at[0], lsem.at[6]),
+        pltpu.make_async_copy(fb_hbm, biases.at[1], lsem.at[6]),
+        pltpu.make_async_copy(q_hbm, query, lsem.at[7]),
+        pltpu.make_async_copy(wo_hbm, wo, lsem.at[8]),
     ]
 
     def arrived(ref, sem):
@@ -109,10 +146,10 @@
         dest = far_to(i)
         late = jnp.where(edge, 0, turns)
         return pltpu.make_async_remote_copy(
-            src_ref=prompt.at[dest * seqs + tp],
+            src_ref=xall.at[dest * seqs + tp],
             dst_ref=xfar.at[tp, local],
             send_sem=sent.at[0],
-            recv_sem=frecv.at[late + i // 2],
+            recv_sem=frecv.at[late + i % turns],
             device_id={"sp": dest},
             device_id_type=MESH,
         )
@@ -154,7 +191,7 @@
             src_ref=piece,
             dst_ref=piece,
             send_sem=sent.at[3],
-            recv_sem=xrecv.at[j, k],
+            recv_sem=xrecv.at[k],
             device_id={"tp": lax.rem(x + j, chips) * cores + c},
             device_id_type=MESH,
         )
@@ -166,7 +203,7 @@
             src_ref=piece,
             dst_ref=piece,
             send_sem=sent.at[4],
-            recv_sem=drecv.at[k],
+            recv_sem=drecv.at[k // 2],
             device_id={"tp": partner},
             device_id_type=MESH,
         )
@@ -189,10 +226,9 @@
     for copy in weight_loads + late_loads:
         copy.start()
 
-    for copy in gate_loads:
-        copy.wait()
+    arrived(gate_w, lsem.at[4])
     wg[...] = jnp.concatenate(
-        [in_gate[...].astype(F32), forget_gate[...].astype(F32), jnp.zeros((wg.shape[0] - 4, depth), F32)],
+        [gate_w[0].astype(F32), gate_w[1].astype(F32), jnp.zeros((wg.shape[0] - 4, depth), F32)],
         axis=0,
     ).astype(BF16)
 
@@ -201,7 +237,7 @@
 
     def gates(start, stop):
         for i in range(start, stop):
-            if i % (2 * half // pieces) == 0:
+            if i < half and i % (2 * half // pieces) == 0:
                 load(i // (2 * half // pieces)).wait()
             dest = (near_base if i < half else far_base) + i % half
             gsend[pl.ds(dest, 1)] = nt(wg[...], rows_of(dest))[:4][None]
@@ -209,6 +245,8 @@
     gates(0, half)
     pl.semaphore_wait(barrier, n - 1 + tpn - 1)
     inner = jnp.logical_not(edge)
+    for i in range(pieces // 2, pieces):
+        load(i).wait()
 
     @pl.when(edge)
     def _():
@@ -219,8 +257,7 @@
     grecv[pl.ds(sp, 1)] = gsend[pl.ds(sp, 1)]
     for k in range(1, n):
         send_gates(k).start()
-    for copy in weight_loads:
-        copy.wait()
+    arrived(wkv, lsem.at[5])
 
     def keys_values(dest):
         return jnp.dot(rows_of(dest), wkv[...], preferred_element_type=F32).astype(BF16)
@@ -252,7 +289,7 @@
             & (iota((2 * n, 2 * n), 1) < iota((2 * n, 2 * n), 0))
         ).astype(F32)
         pre = [
-            grecv[:, i, :] + (in_bias if i < 2 else forget_bias)[0:1, i % 2 : i % 2 + 1]
+            grecv[:, i, :] + biases[i // 2, 0:1, i % 2 : i % 2 + 1]
             for i in range(4)
         ]
         forget_pre = jnp.concatenate(pre[2:], axis=0)
@@ -315,49 +352,51 @@
         for i, source in enumerate(found):
             kvf[pl.ds(source, 1)] = both[i * rows : (i + 1) * rows][None]
 
-    def own(p):
-        for k in (2 * p, 2 * p + 1):
-            arrived(xfar.at[0, 0], frecv.at[k])
-            for j in (2, 1, 3):
-                spread(j, k).start()
-            hand(0, k).start()
-
-    def pass_on(p):
-        for k in (2 * p, 2 * p + 1):
-            for j in (1, 3, 2):
-                arrived(xfar.at[0, 0], xrecv.at[j, k])
-                hand(j, k).start()
+    def own(k):
+        arrived(xfar.at[0, 0], frecv.at[k])
+        for j in (2, 1, 3):
+            spread(j, k).start()
+        hand(0, k).start()
+
+    def pass_on(k):
+        arrived(xfar.at[pl.ds(1, chips - 1), 0], xrecv.at[k])
+        for j in (1, 3, 2):
+            hand(j, k).start()
 
     def collect(p):
-        for k in (2 * p, 2 * p + 1):
-            arrived(xfar.at[0, pl.ds(0, chips)], drecv.at[k])
+        arrived(xfar.at[pl.ds(0, chips), pl.ds(0, 2)], drecv.at[p])
         project(p)
 
-    own(0)
-    for copy in late_loads:
-        copy.wait()
-    turned = query[...].astype(F32).T
-    for q in range(seqs):
-        qb[q] = jnp.broadcast_to(turned[:, q : q + 1], (width, width))
-    arrived(grecv.at[pl.ds(0, n - 1)], recv.at[1])
-    stable = weigh()
-    own(1)
-    widen(0)
-    widen(1)
-    pass_on(0)
-    own(2)
-    widen(2)
-    widen(3)
-    pass_on(1)
-    collect(0)
-    pass_on(2)
-    arrived(kvn.at[pl.ds(0, half - 1)], recv.at[0])
-    for q in range(seqs):
-        acc[q], sums = outer(kvn, 0, q)
-        for g in range(2):
-            nrm[g, q : q + 1] = sums[g]
-    collect(1)
-    collect(2)
+    def queries():
+        arrived(biases, lsem.at[6])
+        for copy in late_loads[2:]:
+            copy.wait()
+        turned = query[...].astype(F32).T
+        for q in range(seqs):
+            qb[q] = jnp.broadcast_to(turned[:, q : q + 1], (width, width))
+
+    stables = []
+
+    def gates_in():
+        arrived(grecv.at[pl.ds(0, n - 1)], recv.at[1])
+        stables.extend(weigh())
+
+    def widened(i):
+        widen(i)
+
+    def near_part():
+        arrived(kvn.at[pl.ds(0, half - 1)], recv.at[0])
+        for q in range(seqs):
+            acc[q], sums = outer(kvn, 0, q)
+            for g in range(2):
+                nrm[g, q : q + 1] = sums[g]
+
+    jobs = {
+        "own": own, "pass": pass_on, "collect": collect, "widen": widened,
+        "queries": lambda _: queries(), "gates": lambda _: gates_in(), "near": lambda _: near_part(),
+    }
+    for job, at in ORDER:
+        jobs[job](at)
     arrived(kvf.at[pl.ds(0, 2)], recv.at[3])
     for q in range(seqs):
         more, sums = outer(kvf, 1, q)
@@ -376,10 +415,10 @@
     queries = query[...].astype(F32)
     for g in range(2):
         under = jnp.abs(jnp.sum(queries * nrm[g], axis=1, keepdims=True))
-        floor = jnp.maximum(jnp.exp(-stable[g]), 1.0)
+        floor = jnp.maximum(jnp.exp(-stables[g]), 1.0)
         hidden = hidden + num[g] / jnp.maximum(under, floor)
         square = iota((seqs, width), 1) == iota((seqs, width), 0)
-        row = jnp.sum(jnp.where(square, stable[g], 0.0), axis=0, keepdims=True)
+        row = jnp.sum(jnp.where(square, stables[g], 0.0), axis=0, keepdims=True)
         stab_out[g] = row[:, :seqs]
     terms = jnp.dot(hidden.astype(BF16), wo[...], preferred_element_type=F32)
     share = terms.shape[1] // tpn
@@ -442,10 +481,8 @@
                 pltpu.VMEM((n * seqs, block, depth), BF16),
                 pltpu.VMEM((depth, 2 * width), BF16),
                 pltpu.VMEM((width, columns), BF16),
-                pltpu.VMEM((2, depth), BF16),
-                pltpu.VMEM((2, depth), BF16),
-                pltpu.VMEM((1, 2), F32),
-                pltpu.VMEM((1, 2), F32),
+                pltpu.VMEM((2, 2, depth), BF16),
+                pltpu.VMEM((2, 1, 2), F32),
                 pltpu.VMEM((seqs, width), BF16),
                 pltpu.VMEM((16, depth), BF16),
                 pltpu.VMEM((half + 1, rows, 2 * width), BF16),
@@ -462,10 +499,10 @@
                 pltpu.VMEM((2, seqs, width), F32),
                 pltpu.VMEM((tpn, seqs, columns // tpn), F32),
                 pltpu.VMEM((tpn, seqs, columns // tpn), F32),
-                dma((12,)),
+                dma((9,)),
                 dma((steps,)),
-                dma((chips, steps)),
                 dma((steps,)),
+                dma((steps // 2,)),
                 dma((4,)),
                 dma((6,)),
             ],

time: 33.2 us -> 31.2 us (0.940)
  Pallas kernels: 32.4 us -> 30.5 us
    pallas_call x1, Pallas kernels: 31.6 us -> 29.6 us  [body(): pl.pallas_call(functools.partial(kernel, n, tpn), out_shape=tuple((pltpu....]
where the time goes in v4:
time: 31.2 us; the launch traced here: 31.1 us
  Pallas kernels  30.5 us (98%)
  between operations  0.64 us (2%)
    pallas_call x1, Pallas kernels, body(): pl.pallas_call(functools.partial(kernel, n, tpn), out_shape=tuple((pltpu....  29.6 us
    pallas_call x1, Pallas kernels, body(): pl.pallas_call(functools.partial(publish, len(shapes)), out_shape=tuple((...  0.84 us

profile of v4, /device:TPU:1, one launch (start us, length us, event | category | flops | bytes accessed | tf_op | source)
XLA Modules:
  0.0 31.1 jit_solution(16593962919880725670)
XLA Ops:
  0.6 29.6 %memories.1 = (bf16[2,8,1,128,128]{4,3,2,1,0:T(8,128)(2,1)S(1)}, f32[2,8,1,128]{3,2,1,0:T(1,128)S(1)}, f32[2,1,8]{2,1,0:T(1,128)S(1)}, bf16[8,128]{1,0:T(8,128)(2,1)S(1)}) custom-call(bf16[128,16,1024]{2,1,0:T(8,128)(2,1)} %prompt.1, bf16[1024,128]{1,0:T(8,128)(2,1)} %bitcast.11, bf16[1024,128]{1,0:T(8,128)(2,1)} %bitcast.12, bf16[128,1024]{1,0:T(8,128)(2,1)} %bitcast.13, ...), custom_call_target="tpu_custom_call" | custom-call | tf_op jit(solution)/shard_map/memories/pallas_call | solution.py:475
  30.3 0.8 %outputs.1 = (bf16[2,8,1,128,128]{4,3,2,1,0:T(8,128)(2,1)}, f32[2,8,1,128]{3,2,1,0:T(1,128)}, f32[2,1,8]{2,1,0:T(1,128)}, bf16[8,128]{1,0:T(8,128)(2,1)}) custom-call(bf16[2,8,1,128,128]{4,3,2,1,0:T(8,128)(2,1)S(1)} %get-tuple-element.12.refs_0_, f32[2,8,1,128]{3,2,1,0:T(1,128)S(1)} %get-tuple-element.13.refs_1_, f32[2,1,8]{2,1,0:T(1,128)S(1)} %get-tuple-element.14.refs_2_, ...), custom_call_target="tpu_custom_call" | custom-call | tf_op jit(solution)/shard_map/outputs/pallas_call | solution.py:516

commit v5 on v4

--- a/solution.py
+++ b/solution.py
@@ -25,7 +25,26 @@
     return lax.broadcasted_iota(jnp.int32, shape, axis)
 
 
-NEAR_ORDER = ("far", 0, 1, 4, 2, 5, 3, 6)
+EDGE_TURNS = (0, 2, 1, 3)
+RAW_TURNS = (2, 3)
+LINE_TURNS = (0, 1)
+FIRST = (
+    ("gates", 0),
+    ("gates", 1),
+    ("barrier", 0),
+    ("loaded", 0),
+    ("edge", 0),
+    ("gates", 2),
+    ("gates", 3),
+    ("send", 0),
+    ("edge", 1),
+    ("weights", 0),
+    ("inner", 0),
+    ("same", 0),
+    ("other", 0),
+    ("line", 0),
+    ("own", 0),
+)
 ORDER = (
     ("own", 0),
     ("own", 1),
@@ -34,20 +53,20 @@
     ("own", 3),
     ("pass", 0),
     ("own", 4),
+    ("pass", 1),
     ("own", 5),
-    ("pass", 1),
+    ("pass", 2),
     ("gates", 0),
-    ("pass", 2),
+    ("pass", 3),
     ("widen", 0),
     ("widen", 1),
-    ("pass", 3),
     ("widen", 2),
+    ("pass", 4),
     ("widen", 3),
     ("collect", 0),
+    ("pass", 5),
+    ("collect", 1),
     ("near", 0),
-    ("pass", 4),
-    ("collect", 1),
-    ("pass", 5),
     ("collect", 2),
 )
 
@@ -98,24 +117,19 @@
             barrier, inc=1, device_id={"tp": lax.rem(tp + j, tpn)}, device_id_type=MESH
         )
 
-    turns = line - 1
-    steps = 2 * turns
-
-    def turn_of(i):
-        return (line // 2, 1, line - 1)[i]
+    first, steps = len(EDGE_TURNS), len(EDGE_TURNS) + len(RAW_TURNS)
 
     def far_from(k):
-        deck_of = 1 - side if k < turns else side
-        return deck_of * line + lax.rem(y + line - turn_of(k % turns), line)
-
-    def far_to(i):
-        deck_of = 1 - side if i < turns else side
-        return far_base + deck_of * line + lax.rem(y + turn_of(i % turns), line)
-
-    def near_to(k):
-        deck_of = 1 - deck if k < line else deck
-        turn = k if k < line else k + 1
-        return near_base + deck_of * line + lax.rem(y + turn, line)
+        deck_of = 1 - side if k < first else side
+        turn = (EDGE_TURNS + RAW_TURNS)[k]
+        return deck_of * line + lax.rem(y + line - turn, line)
+
+    def far_to(i, turns):
+        deck_of = 1 - side if i < len(turns) else side
+        return far_base + deck_of * line + lax.rem(y + turns[i % len(turns)], line)
+
+    def near_to(deck_of, turn):
+        return deck_of * line + lax.rem(y + turn, line)
 
     pieces = 4
 
@@ -142,35 +156,43 @@
     def arrived(ref, sem):
         pltpu.make_async_copy(ref, ref, sem).wait()
 
-    def send_far(i):
-        dest = far_to(i)
-        late = jnp.where(edge, 0, turns)
+    def send_far(i, turns, base):
+        dest = far_to(i, turns)
         return pltpu.make_async_remote_copy(
             src_ref=xall.at[dest * seqs + tp],
             dst_ref=xfar.at[tp, local],
             send_sem=sent.at[0],
-            recv_sem=frecv.at[late + i % turns],
+            recv_sem=frecv.at[base + i % len(turns)],
             device_id={"sp": dest},
             device_id_type=MESH,
         )
 
-    def send_near(k):
-        return pltpu.make_async_remote_copy(
-            src_ref=kvs.at[k],
+    def far_from_edge(at):
+        for i in range(at * first, (at + 1) * first):
+            send_far(i, EDGE_TURNS, 0).start()
+
+    def far_from_inner():
+        for i in range(2 * len(RAW_TURNS)):
+            send_far(i, RAW_TURNS, first).start()
+
+    def send_near(deck_of, turn):
+        dest = near_to(deck_of, turn)
+        return pltpu.make_async_remote_copy(
+            src_ref=kvs.at[dest],
             dst_ref=kvn.at[local],
             send_sem=sent.at[1],
             recv_sem=recv.at[0],
-            device_id={"sp": near_to(k)},
+            device_id={"sp": near_base + dest},
             device_id_type=MESH,
         )
 
     def send_line(i):
         return pltpu.make_async_remote_copy(
-            src_ref=kvs.at[half - 1 + i],
+            src_ref=kvs.at[half + i],
             dst_ref=kvf.at[local],
-            send_sem=sent.at[1],
+            send_sem=sent.at[6],
             recv_sem=recv.at[3],
-            device_id={"sp": far_base + i * line + y},
+            device_id={"sp": far_to(i, LINE_TURNS)},
             device_id_type=MESH,
         )
 
@@ -242,41 +264,56 @@
             dest = (near_base if i < half else far_base) + i % half
             gsend[pl.ds(dest, 1)] = nt(wg[...], rows_of(dest))[:4][None]
 
-    gates(0, half)
-    pl.semaphore_wait(barrier, n - 1 + tpn - 1)
     inner = jnp.logical_not(edge)
-    for i in range(pieces // 2, pieces):
-        load(i).wait()
-
-    @pl.when(edge)
-    def _():
-        for i in range(steps):
-            send_far(i).start()
-
-    gates(half, 2 * half)
-    grecv[pl.ds(sp, 1)] = gsend[pl.ds(sp, 1)]
-    for k in range(1, n):
-        send_gates(k).start()
-    arrived(wkv, lsem.at[5])
-
-    def keys_values(dest):
-        return jnp.dot(rows_of(dest), wkv[...], preferred_element_type=F32).astype(BF16)
-
-    for k in NEAR_ORDER:
-        if k == "far":
-
-            @pl.when(inner)
-            def _():
-                for i in range(steps):
-                    send_far(i).start()
-
-            continue
-        kvs[k] = keys_values(near_to(k))
-        send_near(k).start()
-    for i in range(2):
-        kvs[half - 1 + i] = keys_values(far_base + i * line + y)
-        send_line(i).start()
-    kvn[pl.ds(local, 1)] = keys_values(near_to(half - 1))[None]
+
+    def start_gates():
+        grecv[pl.ds(sp, 1)] = gsend[pl.ds(sp, 1)]
+        for k in range(1, n):
+            send_gates(k).start()
+
+    def keys_values(blocks, base):
+        lines = [rows_of(dest) for dest in blocks]
+        both = jnp.dot(
+            jnp.concatenate(lines, axis=0), wkv[...], preferred_element_type=F32
+        ).astype(BF16)
+        kvs[pl.ds(base, len(blocks))] = both.reshape(len(blocks), rows, 2 * width)
+
+    def near_other():
+        base = (1 - deck) * line
+        keys_values([near_base + base + i for i in range(line)], base)
+        for turn in (2, 1, 3, 0):
+            send_near(1 - deck, turn).start()
+
+    def near_same():
+        base = deck * line
+        keys_values([near_base + base + i for i in range(line)], base)
+        for turn in (2, 1, 3):
+            send_near(deck, turn).start()
+
+    def own_near():
+        kvn[pl.ds(local, 1)] = kvs[pl.ds(local, 1)]
+
+    def lines():
+        count = 2 * len(LINE_TURNS)
+        keys_values([far_to(i, LINE_TURNS) for i in range(count)], half)
+        for i in range(count):
+            send_line(i).start()
+
+    first_jobs = {
+        "barrier": lambda _: pl.semaphore_wait(barrier, n - 1 + tpn - 1),
+        "loaded": lambda _: [load(i).wait() for i in range(pieces // 2, pieces)],
+        "edge": lambda at: pl.when(edge)(functools.partial(far_from_edge, at)),
+        "inner": lambda _: pl.when(inner)(far_from_inner),
+        "gates": lambda at: gates(at * half // 2, (at + 1) * half // 2),
+        "send": lambda _: start_gates(),
+        "weights": lambda _: arrived(wkv, lsem.at[5]),
+        "other": lambda _: near_other(),
+        "same": lambda _: near_same(),
+        "own": lambda _: own_near(),
+        "line": lambda _: pl.when(inner)(lines),
+    }
+    for job, at in FIRST:
+        first_jobs[job](at)
 
     def weigh():
         lane = iota((rows, rows), 1)
@@ -397,7 +434,7 @@
     }
     for job, at in ORDER:
         jobs[job](at)
-    arrived(kvf.at[pl.ds(0, 2)], recv.at[3])
+    arrived(kvf.at[pl.ds(0, len(LINE_TURNS))], recv.at[3])
     for q in range(seqs):
         more, sums = outer(kvf, 1, q)
         memory = (acc[q] + more).astype(BF16)
@@ -426,8 +463,16 @@
         parts[t] = terms[:, t * share : (t + 1) * share]
     for j in range(1, tpn):
         give(j).start()
-    arrived(xfar.at[0, pl.ds(0, steps)], sent.at[0])
-    arrived(kvs, sent.at[1])
+    @pl.when(edge)
+    def _():
+        arrived(xfar.at[0, pl.ds(0, 2 * first)], sent.at[0])
+
+    @pl.when(inner)
+    def _():
+        arrived(xfar.at[0, pl.ds(0, 2 * len(RAW_TURNS))], sent.at[0])
+        arrived(kvs.at[pl.ds(0, 2 * len(LINE_TURNS))], sent.at[6])
+
+    arrived(kvs.at[pl.ds(0, half - 1)], sent.at[1])
     arrived(grecv.at[pl.ds(0, n - 1)], sent.at[2])
     arrived(xfar.at[pl.ds(0, chips - 1), pl.ds(0, steps)], sent.at[3])
     arrived(xfar.at[pl.ds(0, chips), pl.ds(0, steps)], sent.at[4])
@@ -460,7 +505,7 @@
         rows = seqs * block
         half = n // 2
         chips = tpn // 2
-        steps = 2 * (half // 2 - 1)
+        steps = len(EDGE_TURNS) + len(RAW_TURNS)
         wo = w_out.reshape(heads * width, -1)
         columns = wo.shape[1]
         any_ = pl.BlockSpec(memory_space=pl.ANY)
@@ -485,7 +530,7 @@
                 pltpu.VMEM((2, 1, 2), F32),
                 pltpu.VMEM((seqs, width), BF16),
                 pltpu.VMEM((16, depth), BF16),
-                pltpu.VMEM((half + 1, rows, 2 * width), BF16),
+                pltpu.VMEM((half + 2 * len(LINE_TURNS), rows, 2 * width), BF16),
                 pltpu.VMEM((half, rows, 2 * width), BF16),
                 pltpu.VMEM((half, rows, 2 * width), BF16),
                 pltpu.VMEM((n, 4, rows), F32),
@@ -504,7 +549,7 @@
                 dma((steps,)),
                 dma((steps // 2,)),
                 dma((4,)),
-                dma((6,)),
+                dma((7,)),
             ],
             compiler_params=pltpu.CompilerParams(collective_id=0, has_side_effects=True),
             name="memories",

time: 31.2 us -> 31 us (level)
  Pallas kernels: 30.5 us -> 30.1 us
    pallas_call x1, Pallas kernels: 29.6 us -> 29.3 us  [body(): pl.pallas_call(functools.partial(kernel, n, tpn), out_shape=tuple((pltpu....]
where the time goes in v5:
time: 31 us; the launch traced here: 30.7 us
  Pallas kernels  30.1 us (97%)
  between operations  0.64 us (2%)
    pallas_call x1, Pallas kernels, body(): pl.pallas_call(functools.partial(kernel, n, tpn), out_shape=tuple((pltpu....  29.3 us
    pallas_call x1, Pallas kernels, body(): pl.pallas_call(functools.partial(publish, len(shapes)), out_shape=tuple((...  0.84 us

profile of v5, /device:TPU:1, one launch (start us, length us, event | category | flops | bytes accessed | tf_op | source)
XLA Modules:
  0.0 30.7 jit_solution(17373308842328067812)
XLA Ops:
  0.6 29.3 %memories.1 = (bf16[2,8,1,128,128]{4,3,2,1,0:T(8,128)(2,1)S(1)}, f32[2,8,1,128]{3,2,1,0:T(1,128)S(1)}, f32[2,1,8]{2,1,0:T(1,128)S(1)}, bf16[8,128]{1,0:T(8,128)(2,1)S(1)}) custom-call(bf16[128,16,1024]{2,1,0:T(8,128)(2,1)} %prompt.1, bf16[1024,128]{1,0:T(8,128)(2,1)} %bitcast.11, bf16[1024,128]{1,0:T(8,128)(2,1)} %bitcast.12, bf16[128,1024]{1,0:T(8,128)(2,1)} %bitcast.13, ...), custom_call_target="tpu_custom_call" | custom-call | tf_op jit(solution)/shard_map/memories/pallas_call | solution.py:520
  29.9 0.8 %outputs.1 = (bf16[2,8,1,128,128]{4,3,2,1,0:T(8,128)(2,1)}, f32[2,8,1,128]{3,2,1,0:T(1,128)}, f32[2,1,8]{2,1,0:T(1,128)}, bf16[8,128]{1,0:T(8,128)(2,1)}) custom-call(bf16[2,8,1,128,128]{4,3,2,1,0:T(8,128)(2,1)S(1)} %get-tuple-element.12.refs_0_, f32[2,8,1,128]{3,2,1,0:T(1,128)S(1)} %get-tuple-element.13.refs_1_, f32[2,1,8]{2,1,0:T(1,128)S(1)} %get-tuple-element.14.refs_2_, ...), custom_call_target="tpu_custom_call" | custom-call | tf_op jit(solution)/shard_map/outputs/pallas_call | solution.py:561

commit v6 on v5

--- a/solution.py
+++ b/solution.py
@@ -26,23 +26,24 @@
 
 
 EDGE_TURNS = (0, 2, 1, 3)
-RAW_TURNS = (2, 3)
-LINE_TURNS = (0, 1)
+RAW_TO_END, RAW_TO_MIDDLE = (2, 3), (2,)
+LINE_TO_END, LINE_TO_MIDDLE = (0, 1), (0, 1, 3)
+GROUPS = ((0, 1), (2, 3), (4,), (5,))
 FIRST = (
     ("gates", 0),
     ("gates", 1),
     ("barrier", 0),
     ("loaded", 0),
     ("edge", 0),
+    ("edge", 1),
+    ("inner", 0),
     ("gates", 2),
     ("gates", 3),
     ("send", 0),
-    ("edge", 1),
     ("weights", 0),
-    ("inner", 0),
+    ("line", 0),
     ("same", 0),
     ("other", 0),
-    ("line", 0),
     ("own", 0),
 )
 ORDER = (
@@ -66,8 +67,9 @@
     ("collect", 0),
     ("pass", 5),
     ("collect", 1),
+    ("collect", 2),
+    ("collect", 3),
     ("near", 0),
-    ("collect", 2),
 )
 
 
@@ -117,16 +119,20 @@
             barrier, inc=1, device_id={"tp": lax.rem(tp + j, tpn)}, device_id_type=MESH
         )
 
-    first, steps = len(EDGE_TURNS), len(EDGE_TURNS) + len(RAW_TURNS)
+    first = len(EDGE_TURNS)
+    steps, shared = first + len(RAW_TO_END), first + len(RAW_TO_MIDDLE)
 
     def far_from(k):
         deck_of = 1 - side if k < first else side
-        turn = (EDGE_TURNS + RAW_TURNS)[k]
+        turn = (EDGE_TURNS + RAW_TO_END)[k]
         return deck_of * line + lax.rem(y + line - turn, line)
 
-    def far_to(i, turns):
-        deck_of = 1 - side if i < len(turns) else side
-        return far_base + deck_of * line + lax.rem(y + turns[i % len(turns)], line)
+    def far_to(near_middle, turn):
+        deck_of = side if near_middle else 1 - side
+        return far_base + deck_of * line + lax.rem(y + turn, line)
+
+    raw_to = [(False, turn) for turn in RAW_TO_END] + [(True, turn) for turn in RAW_TO_MIDDLE]
+    line_to = [(False, turn) for turn in LINE_TO_END] + [(True, turn) for turn in LINE_TO_MIDDLE]
 
     def near_to(deck_of, turn):
         return deck_of * line + lax.rem(y + turn, line)
@@ -156,24 +162,24 @@
     def arrived(ref, sem):
         pltpu.make_async_copy(ref, ref, sem).wait()
 
-    def send_far(i, turns, base):
-        dest = far_to(i, turns)
+    def send_far(near_middle, turn, slot):
+        dest = far_to(near_middle, turn)
         return pltpu.make_async_remote_copy(
             src_ref=xall.at[dest * seqs + tp],
             dst_ref=xfar.at[tp, local],
             send_sem=sent.at[0],
-            recv_sem=frecv.at[base + i % len(turns)],
+            recv_sem=frecv.at[slot],
             device_id={"sp": dest},
             device_id_type=MESH,
         )
 
     def far_from_edge(at):
-        for i in range(at * first, (at + 1) * first):
-            send_far(i, EDGE_TURNS, 0).start()
+        for slot, turn in enumerate(EDGE_TURNS):
+            send_far(at == 1, turn, slot).start()
 
     def far_from_inner():
-        for i in range(2 * len(RAW_TURNS)):
-            send_far(i, RAW_TURNS, first).start()
+        for i, (near_middle, turn) in enumerate(raw_to):
+            send_far(near_middle, turn, first + i % len(RAW_TO_END)).start()
 
     def send_near(deck_of, turn):
         dest = near_to(deck_of, turn)
@@ -192,7 +198,7 @@
             dst_ref=kvf.at[local],
             send_sem=sent.at[6],
             recv_sem=recv.at[3],
-            device_id={"sp": far_to(i, LINE_TURNS)},
+            device_id={"sp": far_to(*line_to[i])},
             device_id_type=MESH,
         )
 
@@ -218,6 +224,9 @@
             device_id_type=MESH,
         )
 
+    def group_of(k):
+        return [p for p, group in enumerate(GROUPS) if k in group][0]
+
     def hand(j, k):
         origin = lax.rem(x + chips - j, chips) * cores + c
         piece = xfar.at[origin, far_from(k)]
@@ -225,7 +234,7 @@
             src_ref=piece,
             dst_ref=piece,
             send_sem=sent.at[4],
-            recv_sem=drecv.at[k // 2],
+            recv_sem=drecv.at[group_of(k)],
             device_id={"tp": partner},
             device_id_type=MESH,
         )
@@ -294,8 +303,8 @@
         kvn[pl.ds(local, 1)] = kvs[pl.ds(local, 1)]
 
     def lines():
-        count = 2 * len(LINE_TURNS)
-        keys_values([far_to(i, LINE_TURNS) for i in range(count)], half)
+        count = len(line_to)
+        keys_values([far_to(*to) for to in line_to], half)
         for i in range(count):
             send_line(i).start()
 
@@ -381,7 +390,7 @@
         return tn(keys, weighted), sums
 
     def project(p):
-        found = [far_from(2 * p), far_from(2 * p + 1)]
+        found = [far_from(k) for k in GROUPS[p]]
         lines = [xfar[:, pl.ds(source, 1)].reshape(rows, depth) for source in found]
         both = jnp.dot(
             jnp.concatenate(lines, axis=0), wkv[...], preferred_element_type=F32
@@ -401,7 +410,7 @@
             hand(j, k).start()
 
     def collect(p):
-        arrived(xfar.at[pl.ds(0, chips), pl.ds(0, 2)], drecv.at[p])
+        arrived(xfar.at[pl.ds(0, chips), pl.ds(0, len(GROUPS[p]))], drecv.at[p])
         project(p)
 
     def queries():
@@ -433,8 +442,19 @@
         "queries": lambda _: queries(), "gates": lambda _: gates_in(), "near": lambda _: near_part(),
     }
     for job, at in ORDER:
-        jobs[job](at)
-    arrived(kvf.at[pl.ds(0, len(LINE_TURNS))], recv.at[3])
+        slot = GROUPS[at][0] if job == "collect" else at if job in ("own", "pass") else 0
+        if slot < shared:
+            jobs[job](at)
+        else:
+            pl.when(edge)(functools.partial(jobs[job], at))
+    @pl.when(edge)
+    def _():
+        arrived(kvf.at[pl.ds(0, len(LINE_TO_END))], recv.at[3])
+
+    @pl.when(inner)
+    def _():
+        arrived(kvf.at[pl.ds(0, len(LINE_TO_MIDDLE))], recv.at[3])
+
     for q in range(seqs):
         more, sums = outer(kvf, 1, q)
         memory = (acc[q] + more).astype(BF16)
@@ -463,19 +483,23 @@
         parts[t] = terms[:, t * share : (t + 1) * share]
     for j in range(1, tpn):
         give(j).start()
+    def passed(count):
+        arrived(xfar.at[pl.ds(0, chips - 1), pl.ds(0, count)], sent.at[3])
+        arrived(xfar.at[pl.ds(0, chips), pl.ds(0, count)], sent.at[4])
+
     @pl.when(edge)
     def _():
         arrived(xfar.at[0, pl.ds(0, 2 * first)], sent.at[0])
+        passed(steps)
 
     @pl.when(inner)
     def _():
-        arrived(xfar.at[0, pl.ds(0, 2 * len(RAW_TURNS))], sent.at[0])
-        arrived(kvs.at[pl.ds(0, 2 * len(LINE_TURNS))], sent.at[6])
+        arrived(xfar.at[0, pl.ds(0, len(raw_to))], sent.at[0])
+        arrived(kvs.at[pl.ds(0, len(line_to))], sent.at[6])
+        passed(shared)
 
     arrived(kvs.at[pl.ds(0, half - 1)], sent.at[1])
     arrived(grecv.at[pl.ds(0, n - 1)], sent.at[2])
-    arrived(xfar.at[pl.ds(0, chips - 1), pl.ds(0, steps)], sent.at[3])
-    arrived(xfar.at[pl.ds(0, chips), pl.ds(0, steps)], sent.at[4])
     arrived(got.at[pl.ds(0, tpn - 1)], sent.at[5])
     arrived(got.at[pl.ds(0, tpn - 1)], recv.at[2])
     total = parts[tp]
@@ -505,7 +529,7 @@
         rows = seqs * block
         half = n // 2
         chips = tpn // 2
-        steps = len(EDGE_TURNS) + len(RAW_TURNS)
+        steps = len(EDGE_TURNS) + len(RAW_TO_END)
         wo = w_out.reshape(heads * width, -1)
         columns = wo.shape[1]
         any_ = pl.BlockSpec(memory_space=pl.ANY)
@@ -530,7 +554,7 @@
                 pltpu.VMEM((2, 1, 2), F32),
                 pltpu.VMEM((seqs, width), BF16),
                 pltpu.VMEM((16, depth), BF16),
-                pltpu.VMEM((half + 2 * len(LINE_TURNS), rows, 2 * width), BF16),
+                pltpu.VMEM((half + len(LINE_TO_END + LINE_TO_MIDDLE), rows, 2 * width), BF16),
                 pltpu.VMEM((half, rows, 2 * width), BF16),
                 pltpu.VMEM((half, rows, 2 * width), BF16),
                 pltpu.VMEM((n, 4, rows), F32),
@@ -547,7 +571,7 @@
                 dma((9,)),
                 dma((steps,)),
                 dma((steps,)),
-                dma((steps // 2,)),
+                dma((len(GROUPS),)),
                 dma((4,)),
                 dma((7,)),
             ],

time: 31 us -> 30.6 us (0.987)
  no operation moved by 1% of the time
where the time goes in v6:
time: 30.6 us; the launch traced here: 30.5 us
  Pallas kernels  29.9 us (98%)
  between operations  0.64 us (2%)
    pallas_call x1, Pallas kernels, body(): pl.pallas_call(functools.partial(kernel, n, tpn), out_shape=tuple((pltpu....  29 us
    pallas_call x1, Pallas kernels, body(): pl.pallas_call(functools.partial(publish, len(shapes)), out_shape=tuple((...  0.84 us

profile of v6, /device:TPU:1, one launch (start us, length us, event | category | flops | bytes accessed | tf_op | source)
XLA Modules:
  0.0 30.5 jit_solution(600714190869291065)
XLA Ops:
  0.6 29.0 %memories.1 = (bf16[2,8,1,128,128]{4,3,2,1,0:T(8,128)(2,1)S(1)}, f32[2,8,1,128]{3,2,1,0:T(1,128)S(1)}, f32[2,1,8]{2,1,0:T(1,128)S(1)}, bf16[8,128]{1,0:T(8,128)(2,1)S(1)}) custom-call(bf16[128,16,1024]{2,1,0:T(8,128)(2,1)} %prompt.1, bf16[1024,128]{1,0:T(8,128)(2,1)} %bitcast.11, bf16[1024,128]{1,0:T(8,128)(2,1)} %bitcast.12, bf16[128,1024]{1,0:T(8,128)(2,1)} %bitcast.13, ...), custom_call_target="tpu_custom_call" | custom-call | tf_op jit(solution)/shard_map/memories/pallas_call | solution.py:544
  29.7 0.8 %outputs.1 = (bf16[2,8,1,128,128]{4,3,2,1,0:T(8,128)(2,1)}, f32[2,8,1,128]{3,2,1,0:T(1,128)}, f32[2,1,8]{2,1,0:T(1,128)}, bf16[8,128]{1,0:T(8,128)(2,1)}) custom-call(bf16[2,8,1,128,128]{4,3,2,1,0:T(8,128)(2,1)S(1)} %get-tuple-element.12.refs_0_, f32[2,8,1,128]{3,2,1,0:T(1,128)S(1)} %get-tuple-element.13.refs_1_, f32[2,1,8]{2,1,0:T(1,128)S(1)} %get-tuple-element.14.refs_2_, ...), custom_call_target="tpu_custom_call" | custom-call | tf_op jit(solution)/shard_map/outputs/pallas_call | solution.py:585

commit v7 on v6

--- a/solution.py
+++ b/solution.py
@@ -481,7 +481,7 @@
     share = terms.shape[1] // tpn
     for t in range(tpn):
         parts[t] = terms[:, t * share : (t + 1) * share]
-    for j in range(1, tpn):
+    for j in sorted(range(1, tpn), key=lambda j: abs(j - tpn / 2)):
         give(j).start()
     def passed(count):
         arrived(xfar.at[pl.ds(0, chips - 1), pl.ds(0, count)], sent.at[3])

time: 30.6 us -> 30.5 us (level)
  no operation moved by 1% of the time
where the time goes in v7:
time: 30.5 us; the launch traced here: 30.4 us
  Pallas kernels  29.7 us (97%)
  between operations  0.64 us (2%)
    pallas_call x1, Pallas kernels, body(): pl.pallas_call(functools.partial(kernel, n, tpn), out_shape=tuple((pltpu....  28.9 us
    pallas_call x1, Pallas kernels, body(): pl.pallas_call(functools.partial(publish, len(shapes)), out_shape=tuple((...  0.84 us

profile of v7, /device:TPU:1, one launch (start us, length us, event | category | flops | bytes accessed | tf_op | source)
XLA Modules:
  0.0 30.4 jit_solution(5096821578525987874)
XLA Ops:
  0.6 28.9 %memories.1 = (bf16[2,8,1,128,128]{4,3,2,1,0:T(8,128)(2,1)S(1)}, f32[2,8,1,128]{3,2,1,0:T(1,128)S(1)}, f32[2,1,8]{2,1,0:T(1,128)S(1)}, bf16[8,128]{1,0:T(8,128)(2,1)S(1)}) custom-call(bf16[128,16,1024]{2,1,0:T(8,128)(2,1)} %prompt.1, bf16[1024,128]{1,0:T(8,128)(2,1)} %bitcast.11, bf16[1024,128]{1,0:T(8,128)(2,1)} %bitcast.12, bf16[128,1024]{1,0:T(8,128)(2,1)} %bitcast.13, ...), custom_call_target="tpu_custom_call" | custom-call | tf_op jit(solution)/shard_map/memories/pallas_call | solution.py:544
  29.5 0.8 %outputs.1 = (bf16[2,8,1,128,128]{4,3,2,1,0:T(8,128)(2,1)}, f32[2,8,1,128]{3,2,1,0:T(1,128)}, f32[2,1,8]{2,1,0:T(1,128)}, bf16[8,128]{1,0:T(8,128)(2,1)}) custom-call(bf16[2,8,1,128,128]{4,3,2,1,0:T(8,128)(2,1)S(1)} %get-tuple-element.12.refs_0_, f32[2,8,1,128]{3,2,1,0:T(1,128)S(1)} %get-tuple-element.13.refs_1_, f32[2,1,8]{2,1,0:T(1,128)S(1)} %get-tuple-element.14.refs_2_, ...), custom_call_target="tpu_custom_call" | custom-call | tf_op jit(solution)/shard_map/outputs/pallas_call | solution.py:585

commit v8 on v7

--- a/solution.py
+++ b/solution.py
@@ -474,15 +474,16 @@
         under = jnp.abs(jnp.sum(queries * nrm[g], axis=1, keepdims=True))
         floor = jnp.maximum(jnp.exp(-stables[g]), 1.0)
         hidden = hidden + num[g] / jnp.maximum(under, floor)
-        square = iota((seqs, width), 1) == iota((seqs, width), 0)
-        row = jnp.sum(jnp.where(square, stables[g], 0.0), axis=0, keepdims=True)
-        stab_out[g] = row[:, :seqs]
     terms = jnp.dot(hidden.astype(BF16), wo[...], preferred_element_type=F32)
     share = terms.shape[1] // tpn
     for t in range(tpn):
         parts[t] = terms[:, t * share : (t + 1) * share]
     for j in sorted(range(1, tpn), key=lambda j: abs(j - tpn / 2)):
         give(j).start()
+    for g in range(2):
+        square = iota((seqs, width), 1) == iota((seqs, width), 0)
+        row = jnp.sum(jnp.where(square, stables[g], 0.0), axis=0, keepdims=True)
+        stab_out[g] = row[:, :seqs]
     def passed(count):
         arrived(xfar.at[pl.ds(0, chips - 1), pl.ds(0, count)], sent.at[3])
         arrived(xfar.at[pl.ds(0, chips), pl.ds(0, count)], sent.at[4])

time: 30.5 us -> 30.5 us (level)
  no operation moved by 1% of the time
where the time goes in v8:
time: 30.5 us; the launch traced here: 30.4 us
  Pallas kernels  29.7 us (97%)
  between operations  0.64 us (2%)
    pallas_call x1, Pallas kernels, body(): pl.pallas_call(functools.partial(kernel, n, tpn), out_shape=tuple((pltpu....  28.9 us
    pallas_call x1, Pallas kernels, body(): pl.pallas_call(functools.partial(publish, len(shapes)), out_shape=tuple((...  0.84 us

profile of v8, /device:TPU:1, one launch (start us, length us, event | category | flops | bytes accessed | tf_op | source)
XLA Modules:
  0.0 30.4 jit_solution(9862504990326091304)
XLA Ops:
  0.6 28.9 %memories.1 = (bf16[2,8,1,128,128]{4,3,2,1,0:T(8,128)(2,1)S(1)}, f32[2,8,1,128]{3,2,1,0:T(1,128)S(1)}, f32[2,1,8]{2,1,0:T(1,128)S(1)}, bf16[8,128]{1,0:T(8,128)(2,1)S(1)}) custom-call(bf16[128,16,1024]{2,1,0:T(8,128)(2,1)} %prompt.1, bf16[1024,128]{1,0:T(8,128)(2,1)} %bitcast.11, bf16[1024,128]{1,0:T(8,128)(2,1)} %bitcast.12, bf16[128,1024]{1,0:T(8,128)(2,1)} %bitcast.13, ...), custom_call_target="tpu_custom_call" | custom-call | tf_op jit(solution)/shard_map/memories/pallas_call | solution.py:545
  29.5 0.8 %outputs.1 = (bf16[2,8,1,128,128]{4,3,2,1,0:T(8,128)(2,1)}, f32[2,8,1,128]{3,2,1,0:T(1,128)}, f32[2,1,8]{2,1,0:T(1,128)}, bf16[8,128]{1,0:T(8,128)(2,1)}) custom-call(bf16[2,8,1,128,128]{4,3,2,1,0:T(8,128)(2,1)S(1)} %get-tuple-element.12.refs_0_, f32[2,8,1,128]{3,2,1,0:T(1,128)S(1)} %get-tuple-element.13.refs_1_, f32[2,1,8]{2,1,0:T(1,128)S(1)} %get-tuple-element.14.refs_2_, ...), custom_call_target="tpu_custom_call" | custom-call | tf_op jit(solution)/shard_map/outputs/pallas_call | solution.py:586

commit v9 on v7

--- a/solution.py
+++ b/solution.py
@@ -290,7 +290,7 @@
     def near_other():
         base = (1 - deck) * line
         keys_values([near_base + base + i for i in range(line)], base)
-        for turn in (2, 1, 3, 0):
+        for turn in (0, 2, 1, 3):
             send_near(1 - deck, turn).start()
 
     def near_same():

time: 30.5 us -> 30.4 us (level)
  no operation moved by 1% of the time
where the time goes in v9:
time: 30.4 us; the launch traced here: 30.3 us
  Pallas kernels  29.7 us (98%)
  between operations  0.64 us (2%)
    pallas_call x1, Pallas kernels, body(): pl.pallas_call(functools.partial(kernel, n, tpn), out_shape=tuple((pltpu....  28.8 us
    pallas_call x1, Pallas kernels, body(): pl.pallas_call(functools.partial(publish, len(shapes)), out_shape=tuple((...  0.84 us

profile of v9, /device:TPU:1, one launch (start us, length us, event | category | flops | bytes accessed | tf_op | source)
XLA Modules:
  0.0 30.3 jit_solution(5845815887983898858)
XLA Ops:
  0.6 28.8 %memories.1 = (bf16[2,8,1,128,128]{4,3,2,1,0:T(8,128)(2,1)S(1)}, f32[2,8,1,128]{3,2,1,0:T(1,128)S(1)}, f32[2,1,8]{2,1,0:T(1,128)S(1)}, bf16[8,128]{1,0:T(8,128)(2,1)S(1)}) custom-call(bf16[128,16,1024]{2,1,0:T(8,128)(2,1)} %prompt.1, bf16[1024,128]{1,0:T(8,128)(2,1)} %bitcast.11, bf16[1024,128]{1,0:T(8,128)(2,1)} %bitcast.12, bf16[128,1024]{1,0:T(8,128)(2,1)} %bitcast.13, ...), custom_call_target="tpu_custom_call" | custom-call | tf_op jit(solution)/shard_map/memories/pallas_call | solution.py:544
  29.5 0.8 %outputs.1 = (bf16[2,8,1,128,128]{4,3,2,1,0:T(8,128)(2,1)}, f32[2,8,1,128]{3,2,1,0:T(1,128)}, f32[2,1,8]{2,1,0:T(1,128)}, bf16[8,128]{1,0:T(8,128)(2,1)}) custom-call(bf16[2,8,1,128,128]{4,3,2,1,0:T(8,128)(2,1)S(1)} %get-tuple-element.12.refs_0_, f32[2,8,1,128]{3,2,1,0:T(1,128)S(1)} %get-tuple-element.13.refs_1_, f32[2,1,8]{2,1,0:T(1,128)S(1)} %get-tuple-element.14.refs_2_, ...), custom_call_target="tpu_custom_call" | custom-call | tf_op jit(solution)/shard_map/outputs/pallas_call | solution.py:585
